TPU v7x, 32 devices: a whole 2x2x4 slice. The times are simulated.
32 devices in a mesh: sp: 4 (over z), fs: 4 (over y, x), tp: 2 (over core).
Axes of the slice: x: 2, y: 2, z: 4, core: 2. Of those that a mesh axis runs over, the one named last changes fastest.
Arguments:
- recurrent_query: bfloat16 [4, 1024, 1024], P('fs', 'sp', 'tp'), may hold values from -6 to 6
- forget_logits: bfloat16 [4, 1024, 1024], P('fs', 'sp', 'tp'), may hold values from -6 to 6
- recurrent_value: bfloat16 [4, 1024, 1024], P('fs', 'sp', 'tp'), may hold values from -6 to 6
- forget_floor: float32 [2, 1024], P(None, 'tp'), may hold values from 0.8 to 1
- extra_log_decay: float32 [4, 1024, 8], P('fs', 'sp', 'tp'), may hold values from -1 to 0
- recurrent_norm_gain: float32 [1024], P('tp'), may hold values from 0.1 to 1.9
- attention_query: bfloat16 [4, 1024, 768], P('fs', 'sp', 'tp'), may hold values from -300 to 300
- latent: bfloat16 [4, 1024, 256], P('fs', 'sp'), may hold values from -6 to 6
- rotary_key: bfloat16 [4, 1024, 32], P('fs', 'sp'), may hold values from -15 to 15
- latent_norm_gain: float32 [256], replicated, may hold values from 0.1 to 1.9
- latent_up_weight: bfloat16 [256, 1024], replicated, may hold values from -0.375 to 0.375
- recurrent_output_weight: bfloat16 [1024, 2048], P('tp', 'fs'), may hold values from -0.1875 to 0.1875
- attention_output_weight: bfloat16 [512, 2048], P('tp', 'fs'), may hold values from -2 to 2
Outputs:
- mixed: bfloat16 [4, 1024, 2048], P('fs', ('sp', 'tp'))
- log_weight: float32 [4, 1024, 8], P('fs', 'sp', 'tp')
All inputs are finite; a program needn't handle non-finite values.
Results may differ from a plain program's by a relative error of at most 0.013.
The roundings to bfloat16 on the way count: a program that leaves them out, or rounds other values in their place, can miss the bound.
Values may be sent and summed in bfloat16 or wider, within the bound.
A program may use at most 128 MiB of HBM per device.

v0:
```python
import functools

import jax
import jax.numpy as jnp
import numpy as np
from jax import lax
from jax.experimental import pallas as pl
from jax.experimental.pallas import tpu as pltpu
from jax.sharding import PartitionSpec as P

HG_DK = 128
NOPE = 64
ROPE = 32
VDIM = 64
HEAD = NOPE + ROPE
LANES = 128
BLOCK = 128

norm_eps = 1e-06
rope_base = 10000.0
widest_span = 8

F32 = jnp.float32
BF16 = jnp.bfloat16


def mm(a, b):
    return jnp.dot(a, b, preferred_element_type=F32)


def mm_nt(a, b):
    return lax.dot_general(a, b, (((1,), (1,)), ((), ())), preferred_element_type=F32)


def mm_tn(a, b):
    return lax.dot_general(a, b, (((0,), (0,)), ((), ())), preferred_element_type=F32)


def flip_bits(value, mask):
    bit = 1
    while bit <= mask:
        if mask & bit:
            value = value + bit - 2 * bit * lax.rem(value // bit, 2)
        bit *= 2
    return value


def rope_constants(seq_len, heads):
    half = ROPE // 2
    inverse = (np.float32(rope_base) ** (-np.arange(half, dtype=np.float32) / np.float32(half))).astype(np.float32)
    angles = np.arange(seq_len, dtype=np.float32)[:, None] * inverse[None, :]
    cos_pad = np.zeros((seq_len, LANES), np.float32)
    sin_pad = np.zeros((seq_len, LANES), np.float32)
    cos_pad[:, :NOPE] = 1.0
    cos_pad[:, NOPE:HEAD] = np.tile(np.cos(angles), (1, 2))
    sin_pad[:, NOPE:HEAD] = np.tile(np.sin(angles), (1, 2))
    place = np.zeros((heads * HEAD, heads * LANES), np.float32)
    swap = np.zeros((heads * HEAD, heads * LANES), np.float32)
    for h in range(heads):
        for i in range(HEAD):
            place[h * HEAD + i, h * LANES + i] = 1.0
        for i in range(half):
            a, b = NOPE + i, NOPE + half + i
            swap[h * HEAD + b, h * LANES + a] = -1.0
            swap[h * HEAD + a, h * LANES + b] = 1.0
    return cos_pad, sin_pad, place, swap


def kernel(
    sizes,
    q_ref, f_ref, v_ref, floor_ref, extra_ref, gain_ref, aq_ref, lat_ref, rk_ref,
    lgain_ref, wup_ref, cos_ref, sin_ref, place_ref, swap_ref, w1_ref, w2_ref,
    out_ref, logw_ref,
    lbuf, ssend, srecv, w1buf, w2buf, psend, precv,
    kbuf, vbuf, intra, qf_ref, qb_ref, sf_ref, sb_ref, act, whole_state, whole_decay,
    l_send, l_recv, f_send, f_recv, s_send, s_recv, w_send, w_recv, r_send, r_recv,
    x_send, x_recv, own_sem,
):
    n_fs, span = sizes
    tokens, width = q_ref.shape
    heads = width // HG_DK
    att_heads = aq_ref.shape[1] // HEAD
    up = att_heads * (NOPE + VDIM)
    blocks = tokens // BLOCK
    latent_width = lat_ref.shape[1]
    columns = w1_ref.shape[1]
    rows = tokens // 2

    sp, fs, tp = lax.axis_index("sp"), lax.axis_index("fs"), lax.axis_index("tp")
    place = lax.rem(sp, span)
    base = sp - place

    def sp_peer(j):
        return {"sp": base + lax.rem(place + j, span)}

    def fs_peer(j):
        return {"fs": flip_bits(fs, j)}

    partner = {"tp": 1 - tp}

    barrier = pltpu.get_barrier_semaphore()
    for j in range(1, n_fs):
        pl.semaphore_signal(barrier, inc=1, device_id=fs_peer(j), device_id_type=pl.DeviceIdType.MESH)
    for j in range(1, span):
        pl.semaphore_signal(barrier, inc=1, device_id=sp_peer(j), device_id_type=pl.DeviceIdType.MESH)
    pl.semaphore_signal(barrier, inc=1, device_id=partner, device_id_type=pl.DeviceIdType.MESH)
    pl.semaphore_wait(barrier, n_fs + span - 1)

    def remote(src, dst, send, recv, device):
        return pltpu.make_async_remote_copy(
            src_ref=src, dst_ref=dst, send_sem=send, recv_sem=recv,
            device_id=device, device_id_type=pl.DeviceIdType.MESH,
        )

    parity = lax.rem(place, 2)
    pair = {"sp": base + flip_bits(place, 1)}
    far = [j for j in range(1, n_fs) if j & (j - 1) and span % 2 == 0]
    near = [j for j in range(1, n_fs) if j not in far]
    weights = ((w1_ref, w1buf), (w2_ref, w2buf))

    def half_rows(ref):
        size = ref.shape[-2] // 2
        return pl.ds(pl.multiple_of(parity * size, size), size)

    w_copies = {}
    for j in far + near:
        pieces = []
        for k, (src, dst) in enumerate(weights):
            there = dst.at[j]
            if j in far:
                src, there = src.at[half_rows(src)], there.at[half_rows(dst)]
            c = remote(src, there, w_send.at[2 * j + k], w_recv.at[2 * j + k], fs_peer(j))
            c.start()
            pieces.append(c)
        w_copies[j] = pieces
    relays = {j: [
        remote(dst.at[j, half_rows(dst)], dst.at[j, half_rows(dst)],
               r_send.at[2 * j + k], r_recv.at[2 * j + k], pair)
        for k, (_, dst) in enumerate(weights)
    ] for j in far}
    own = (
        pltpu.make_async_copy(w1_ref, w1buf.at[0], own_sem.at[0]),
        pltpu.make_async_copy(w2_ref, w2buf.at[0], own_sem.at[1]),
    )
    for c in own:
        c.start()

    offset = pl.multiple_of(place * tokens, tokens)
    cos = cos_ref[pl.ds(offset, tokens), :]
    sin = sin_ref[pl.ds(offset, tokens), :]
    lat = lat_ref[...].astype(F32)
    normed = lat * lax.rsqrt(jnp.mean(lat * lat, axis=-1, keepdims=True) + norm_eps) * lgain_ref[...]
    lbuf[0, :, :latent_width] = normed.astype(BF16)
    rk = rk_ref[...]
    rotated = mm_tn(rk, place_ref[NOPE:HEAD, :LANES]) * cos + mm_tn(rk, swap_ref[NOPE:HEAD, :LANES]) * sin
    lbuf[0, :, latent_width:] = rotated.astype(BF16)
    my_rows = pl.ds(pl.multiple_of(tp * rows, rows), rows)
    l_copies = []
    for j in range(1, span):
        c = remote(lbuf.at[0, my_rows], lbuf.at[j, my_rows], l_send.at[j], l_recv.at[j], sp_peer(j))
        c.start()
        l_copies.append(c)

    row = lax.broadcasted_iota(jnp.int32, (BLOCK, BLOCK), 0)
    col = lax.broadcasted_iota(jnp.int32, (BLOCK, BLOCK), 1)
    lower = row >= col
    upper = row <= col
    tri = (jnp.where(lower, 1.0, 0.0).astype(BF16), jnp.where(upper, 1.0, 0.0).astype(BF16))
    spikes = lax.dot_general(
        extra_ref[...],
        jnp.where(
            lax.broadcasted_iota(jnp.int32, (heads, width), 0)
            == lax.broadcasted_iota(jnp.int32, (heads, width), 1) // HG_DK, 1.0, 0.0),
        (((0,), (0,)), ((), ())), precision=lax.Precision.HIGHEST, preferred_element_type=F32)
    block_decay = [[[None] * blocks for _ in range(2)] for _ in range(heads)]
    for h in range(heads):
        lanes = slice(h * HG_DK, (h + 1) * HG_DK)
        for b in range(blocks):
            tok = slice(b * BLOCK, (b + 1) * BLOCK)
            q = q_ref[tok, lanes].astype(F32)
            gate = f_ref[tok, lanes].astype(F32)
            v = v_ref[tok, lanes]
            miss = 1.0 / (1.0 + jnp.exp(gate))
            spike = spikes[tok, lanes]
            scores = None
            for d in range(2):
                keyed = (1.0 - floor_ref[d : d + 1, lanes]) * miss
                decay = jnp.log1p(-keyed) + spike
                hi = decay.astype(BF16)
                lo = (decay - hi.astype(F32)).astype(BF16)
                run = mm(tri[d], hi) + mm(tri[d], lo)
                mid_at = BLOCK // 2 - 1 if d == 0 else BLOCK // 2
                end_at = BLOCK - 1 if d == 0 else 0
                mid = run[mid_at : mid_at + 1]
                end = run[end_at : end_at + 1]
                grow = jnp.exp(run - mid)
                qd = q * grow
                kd = keyed * jnp.exp(mid - run)
                s = mm_nt(qd.astype(BF16), kd.astype(BF16))
                s = jnp.where(lower if d == 0 else upper, s, 0.0)
                scores = s if scores is None else scores + s
                cross = qf_ref if d == 0 else qb_ref
                cross[tok, lanes] = (qd * jnp.exp(mid)).astype(BF16)
                state = mm_tn(v, (kd * jnp.exp(end - mid)).astype(BF16))
                keep = sf_ref if d == 0 else sb_ref
                keep[b, :, lanes] = state
                block_decay[h][d][b] = jnp.exp(end)
            intra[tok, lanes] = mm(scores.astype(BF16), v)
        for d in range(2):
            keep = sf_ref if d == 0 else sb_ref
            order = range(blocks) if d == 0 else range(blocks - 1, -1, -1)
            total, decay_all = None, None
            for b in order:
                one = keep[b, :, lanes]
                dec = block_decay[h][d][b]
                total = one if total is None else total * dec + one
                decay_all = dec if decay_all is None else decay_all * dec
            whole_state[d, h] = total
            whole_decay[d, h] = jnp.broadcast_to(decay_all, (8, HG_DK))

    first = jnp.where(2 * place < span, 0, 1)

    def link(d, h):
        towards = jnp.clip(place + 1 - 2 * d, 0, span - 1)
        return remote(ssend.at[d, h], srecv.at[d, h], s_send.at[d, h], s_recv.at[d, h],
                      {"sp": base + towards})

    def has_previous(d):
        return jnp.where(d == 0, place, span - 1 - place) > 0

    def has_next(d):
        return jnp.where(d == 0, span - 1 - place, place) > 0

    def pass_on(d):
        for h in range(heads):
            @pl.when(has_previous(d))
            def _():
                link(d, h).wait_recv()

            @pl.when(jnp.logical_not(has_previous(d)))
            def _():
                srecv[d, h] = jnp.zeros((HG_DK, HG_DK), BF16)

            @pl.when(has_next(d))
            def _():
                reached = srecv[d, h].astype(F32) * whole_decay[d, h, 0:1] + whole_state[d, h]
                ssend[d, h] = reached.astype(BF16)
                link(d, h).start()

    pass_on(first)

    forwards = []
    for j in range(1, span):
        l_copies[j - 1].wait_recv()
        c = remote(lbuf.at[j, my_rows], lbuf.at[j, my_rows], f_send.at[j], f_recv.at[j], partner)
        c.start()
        forwards.append(c)

    @pl.when(has_next(1 - first))
    def _():
        pass_on(1 - first)

    for j in far:
        for c, r in zip(w_copies[j], relays[j]):
            c.wait_recv()
            r.start()

    tp_up = pl.multiple_of(tp * up, LANES)
    wup = wup_ref[:, pl.ds(tp_up, up)]
    lane = lax.broadcasted_iota(jnp.int32, (tokens, LANES), 1)
    for j in range(span):
        if j > 0:
            forwards[j - 1].wait_recv()
        keys = slice(j * tokens, (j + 1) * tokens)
        expanded = mm(lbuf[j, :, :latent_width], wup)
        rot = lbuf[j, :, latent_width:].astype(F32)
        vbuf[keys, :] = expanded.astype(BF16)
        for h in range(att_heads):
            lanes = slice(h * LANES, (h + 1) * LANES)
            kbuf[keys, lanes] = jnp.where(lane < NOPE, expanded[:, lanes], rot).astype(BF16)
    aq = aq_ref[...]
    scale = HEAD ** (-0.5)
    logw = jnp.zeros((tokens, LANES), F32)
    kept = None
    for h in range(att_heads):
        lanes = slice(h * LANES, (h + 1) * LANES)
        query = mm(aq, place_ref[:, lanes]) * cos + mm(aq, swap_ref[:, lanes]) * sin
        scores = mm_nt(query.astype(BF16), kbuf[:, lanes]) * scale
        peak = jnp.max(scores, axis=-1, keepdims=True)
        weights = jnp.exp(scores - peak)
        totals = jnp.sum(weights, axis=-1, keepdims=True)
        result = mm(weights.astype(BF16), vbuf[:, lanes]) / totals
        logw = jnp.where(lane == h, peak + jnp.log(totals), logw)
        if h % 2 == 0:
            kept = pltpu.roll(result, VDIM, 1)
        else:
            at = width + (h // 2) * LANES
            act[:, at : at + LANES] = jnp.where(lane < VDIM, kept, result).astype(BF16)
    logw_ref[...] = jnp.transpose(logw)[:att_heads]

    @pl.when(jnp.logical_not(has_next(1 - first)))
    def _():
        pass_on(1 - first)

    for h in range(heads):
        lanes = slice(h * HG_DK, (h + 1) * HG_DK)
        carry_f = srecv[0, h].astype(F32)
        carry_b = srecv[1, h].astype(F32)
        starts_f = []
        for b in range(blocks):
            starts_f.append(carry_f)
            carry_f = carry_f * block_decay[h][0][b] + sf_ref[b, :, lanes]
        starts_b = [None] * blocks
        for b in range(blocks - 1, -1, -1):
            starts_b[b] = carry_b
            carry_b = carry_b * block_decay[h][1][b] + sb_ref[b, :, lanes]
        for b in range(blocks):
            tok = slice(b * BLOCK, (b + 1) * BLOCK)
            o = intra[tok, lanes]
            o = o + mm_nt(qf_ref[tok, lanes], starts_f[b].astype(BF16))
            o = o + mm_nt(qb_ref[tok, lanes], starts_b[b].astype(BF16))
            o = o * lax.rsqrt(jnp.mean(o * o, axis=-1, keepdims=True) + norm_eps) * gain_ref[:, lanes]
            act[tok, lanes] = o.astype(BF16)

    mine = pl.multiple_of(tp * rows, rows)
    theirs = pl.multiple_of((1 - tp) * rows, rows)
    kept_rows = []
    x_copies = []

    def finish(j):
        x_copies[j].wait_recv()
        at = pl.multiple_of(flip_bits(fs, j) * columns, LANES)
        out_ref[:, pl.ds(at, columns)] = (kept_rows[j] + precv[j].astype(F32)).astype(BF16)

    for j in range(n_fs):
        if j == 0:
            for c in own:
                c.wait()
        else:
            for c in relays[j] if j in far else w_copies[j]:
                c.wait_recv()
        away = mm(act[pl.ds(theirs, rows), :width], w1buf[j]) + mm(act[pl.ds(theirs, rows), width:], w2buf[j])
        psend[j] = away.astype(BF16)
        c = remote(psend.at[j], precv.at[j], x_send.at[j], x_recv.at[j], partner)
        c.start()
        x_copies.append(c)
        here = mm(act[pl.ds(mine, rows), :width], w1buf[j]) + mm(act[pl.ds(mine, rows), width:], w2buf[j])
        kept_rows.append(here.astype(BF16).astype(F32))
        if j > 0:
            finish(j - 1)
    finish(n_fs - 1)

    for pieces in list(w_copies.values()) + list(relays.values()):
        for c in pieces:
            c.wait_send()
    for c in l_copies + forwards + x_copies:
        c.wait_send()
    for d in range(2):
        for h in range(heads):
            @pl.when(has_next(d))
            def _():
                link(d, h).wait_send()


def local(
    n_fs,
    n_sp,
    recurrent_query,
    forget_logits,
    recurrent_value,
    forget_floor,
    extra_log_decay,
    recurrent_norm_gain,
    attention_query,
    latent,
    rotary_key,
    latent_norm_gain,
    latent_up_weight,
    recurrent_output_weight,
    attention_output_weight,
):
    span = min(n_sp, widest_span)
    tokens, width = recurrent_query.shape[1:]
    heads = width // HG_DK
    att_heads = attention_query.shape[2] // HEAD
    latent_width = latent.shape[2]
    columns = recurrent_output_weight.shape[1]
    att_width = attention_output_weight.shape[0]
    blocks = tokens // BLOCK
    rows = tokens // 2
    cos_pad, sin_pad, place, swap = rope_constants(span * tokens, att_heads)
    vmem = pl.BlockSpec(memory_space=pltpu.VMEM)
    anywhere = pl.BlockSpec(memory_space=pl.ANY)
    dma = pltpu.SemaphoreType.DMA
    mixed, log_weight = pl.pallas_call(
        functools.partial(kernel, (n_fs, span)),
        out_shape=(
            jax.ShapeDtypeStruct((rows, columns * n_fs), BF16),
            jax.ShapeDtypeStruct((att_heads, tokens), F32),
        ),
        in_specs=[vmem] * 15 + [anywhere] * 2,
        out_specs=(vmem, vmem),
        scratch_shapes=[
            pltpu.VMEM((span, tokens, latent_width + LANES), BF16),
            pltpu.VMEM((2, heads, HG_DK, HG_DK), BF16),
            pltpu.VMEM((2, heads, HG_DK, HG_DK), BF16),
            pltpu.VMEM((n_fs, width, columns), BF16),
            pltpu.VMEM((n_fs, att_width, columns), BF16),
            pltpu.VMEM((n_fs, rows, columns), BF16),
            pltpu.VMEM((n_fs, rows, columns), BF16),
            pltpu.VMEM((span * tokens, att_heads * LANES), BF16),
            pltpu.VMEM((span * tokens, att_heads * LANES), BF16),
            pltpu.VMEM((tokens, width), F32),
            pltpu.VMEM((tokens, width), BF16),
            pltpu.VMEM((tokens, width), BF16),
            pltpu.VMEM((blocks, HG_DK, width), F32),
            pltpu.VMEM((blocks, HG_DK, width), F32),
            pltpu.VMEM((tokens, width + att_width), BF16),
            pltpu.VMEM((2, heads, HG_DK, HG_DK), F32),
            pltpu.VMEM((2, heads, 8, HG_DK), F32),
            dma((span,)), dma((span,)), dma((span,)), dma((span,)), dma((2, heads)), dma((2, heads)),
            dma((2 * n_fs,)), dma((2 * n_fs,)), dma((2 * n_fs,)), dma((2 * n_fs,)),
            dma((n_fs,)), dma((n_fs,)), dma((2,)),
        ],
        compiler_params=pltpu.CompilerParams(
            collective_id=0, has_side_effects=True, vmem_limit_bytes=56 * 2**20
        ),
        name="mixers",
    )(
        recurrent_query[0],
        forget_logits[0],
        recurrent_value[0],
        forget_floor,
        extra_log_decay[0].T,
        recurrent_norm_gain[None],
        attention_query[0],
        latent[0],
        rotary_key[0].T,
        latent_norm_gain[None],
        latent_up_weight,
        jnp.asarray(cos_pad),
        jnp.asarray(sin_pad),
        jnp.asarray(place, BF16),
        jnp.asarray(swap, BF16),
        recurrent_output_weight,
        attention_output_weight,
    )
    return mixed[None], log_weight.T[None]


def solution(mesh):
    placed = (
        P("fs", "sp", "tp"),
        P("fs", "sp", "tp"),
        P("fs", "sp", "tp"),
        P(None, "tp"),
        P("fs", "sp", "tp"),
        P("tp"),
        P("fs", "sp", "tp"),
        P("fs", "sp", None),
        P("fs", "sp", None),
        P(),
        P(),
        P("tp", "fs"),
        P("tp", "fs"),
    )
    return jax.shard_map(
        functools.partial(local, mesh.shape["fs"], mesh.shape["sp"]),
        mesh=mesh,
        in_specs=placed,
        out_specs=(P("fs", ("sp", "tp"), None), P("fs", "sp", "tp")),
        check_vma=False,
    )
```

profile of v0, /device:TPU:0, one launch (start us, length us, event | category | flops | bytes accessed | tf_op | source)
XLA Modules:
  0.0 41.9 jit_solution(2199201381174137100)
XLA Ops:
  0.6 38.8 %mixers.1 = (bf16[128,2048]{1,0:T(8,128)(2,1)}, f32[4,256]{1,0:T(4,128)}) custom-call(bf16[256,512]{1,0:T(8,128)(2,1)} %bitcast.18, bf16[256,512]{1,0:T(8,128)(2,1)} %bitcast.19, bf16[256,512]{1,0:T(8,128)(2,1)} %bitcast.20, f32[2,512]{1,0:T(2,128)} %floor_ref.1, f32[4,256]{1,0:T(4,128)} %bitcast.25, f32[1,512]{1,0:T(1,128)} %bitcast.26, ...), custom_call_target="tpu_custom_call" | custom-call | tf_op jit(solution)/shard_map/mixers/pallas_call | solution.py:395
  39.5 0.0 copy-start
  39.5 1.9 %copy.21 = bf16[1,128,2048]{2,1,0:T(8,128)(2,1)} copy(bf16[1,128,2048]{2,1,0:T(8,128)(2,1)} %bitcast.17) | data formatting | bytes 1048576
  41.3 0.0 copy-done
  41.3 0.6 %copy.22 = f32[1,256,4]{1,2,0:T(4,128)} copy(f32[1,256,4]{1,2,0:T(4,128)S(1)} %bitcast.24) | data formatting | bytes 8192
Async XLA Ops:
  39.5 1.9 %copy-start = (f32[4,256]{1,0:T(4,128)S(1)}, f32[4,256]{1,0:T(4,128)}, u32[]{:S(2)}) copy-start(f32[4,256]{1,0:T(4,128)} %get-tuple-element.5) | copy-start | bytes 12292
where the time goes:
time: 42.1 us; the launch traced here: 41.9 us
  Pallas kernels  38.8 us (92%)
  local copies, waits for them, and re-layouts  2.48 us (6%)
  between operations  0.65 us (2%)
    pallas_call x1, Pallas kernels, local(): pl.pallas_call(functools.partial(kernel, (n_fs, span)), out_shape=(jax.Sh...  38.8 us
    unnamed x4, local copies, waits for them, and re-layouts  2.48 us

commit v1 on v0

v1 whole, which is shorter than its diff:
```python
import functools

import jax
import jax.numpy as jnp
import numpy as np
from jax import lax
from jax.experimental import pallas as pl
from jax.experimental.pallas import tpu as pltpu
from jax.sharding import PartitionSpec as P

HG_DK = 128
NOPE = 64
ROPE = 32
VDIM = 64
HEAD = NOPE + ROPE
LANES = 128
BLOCK = 128

norm_eps = 1e-06
rope_base = 10000.0
widest_span = 8

F32 = jnp.float32
BF16 = jnp.bfloat16


def mm(a, b):
    return jnp.dot(a, b, preferred_element_type=F32)


def mm_nt(a, b):
    return lax.dot_general(a, b, (((1,), (1,)), ((), ())), preferred_element_type=F32)


def mm_tn(a, b):
    return lax.dot_general(a, b, (((0,), (0,)), ((), ())), preferred_element_type=F32)


def flip_bits(value, mask):
    bit = 1
    while bit <= mask:
        if mask & bit:
            value = value + bit - 2 * bit * lax.rem(value // bit, 2)
        bit *= 2
    return value


def rope_constants(seq_len, heads):
    half = ROPE // 2
    inverse = (np.float32(rope_base) ** (-np.arange(half, dtype=np.float32) / np.float32(half))).astype(np.float32)
    angles = np.arange(seq_len, dtype=np.float32)[:, None] * inverse[None, :]
    cos_pad = np.zeros((seq_len, LANES), np.float32)
    sin_pad = np.zeros((seq_len, LANES), np.float32)
    cos_pad[:, :NOPE] = 1.0
    cos_pad[:, NOPE:HEAD] = np.tile(np.cos(angles), (1, 2))
    sin_pad[:, NOPE:HEAD] = np.tile(np.sin(angles), (1, 2))
    turns = np.concatenate([np.cos(angles).T, np.sin(angles).T], axis=0)
    place = np.zeros((heads * HEAD, heads * LANES), np.float32)
    swap = np.zeros((heads * HEAD, heads * LANES), np.float32)
    for h in range(heads):
        for i in range(HEAD):
            place[h * HEAD + i, h * LANES + i] = 1.0
        for i in range(half):
            a, b = NOPE + i, NOPE + half + i
            swap[h * HEAD + b, h * LANES + a] = -1.0
            swap[h * HEAD + a, h * LANES + b] = 1.0
    return cos_pad, sin_pad, turns, place, swap


def transfer_plan(n_fs, span, groups, cuts):
    count = groups * cuts
    paired = span % 2 == 0
    if n_fs == 4 and paired:
        direct = count - count // 3
        lists = {1: list(range(direct)), 2: list(range(count - 1, count - 1 - direct, -1))}
        half = count // 2
        cross = [(1, v) for v in range(half)], [(2, v) for v in range(count - 1, half - 1, -1)]
        over = [(1, v) for v in range(count - direct)], [(2, v) for v in range(count - 1, direct - 1, -1)]
        steps = []
        for k in range(half):
            step = [(cross[0][k], "cross"), (cross[1][k], "cross")]
            if k < len(over[0]):
                step += [(over[0][k], "pair"), (over[1][k], "pair")]
            steps.append(step)
        when = {}
        for k in range(direct):
            when[1, lists[1][k]] = when[2, lists[2][k]] = k + 1
        for k in range(half):
            when[3, cross[0][k][1]] = when[3, cross[1][k][1]] = direct + k + 1
        for k in range(count - direct):
            when[1, count - 1 - over[0][k][1]] = 5 + 2 * k
            when[2, count - 1 - over[1][k][1]] = 6 + 2 * k
    else:
        lists = {j: list(range(count)) for j in range(1, n_fs)}
        steps = []
        when = {(j, v): v * n_fs + j for j in lists for v in lists[j]}
    order = [(0, g) for g in range(groups)]
    rest = [(max(when[j, g * cuts + b] for b in range(cuts)), j, g) for j in range(1, n_fs) for g in range(groups)]
    order += [(j, g) for _, j, g in sorted(rest)]
    return lists, steps, order


def kernel(
    sizes,
    q_hbm, f_hbm, v_hbm, floor_hbm, extra_hbm, gain_hbm, aq_hbm, lat_hbm, rk_hbm,
    lgain_hbm, wup_hbm, cos_hbm, sin_hbm, turn_hbm, place_hbm, swap_hbm, w1_hbm, w2_hbm,
    out_hbm, logw_hbm,
    q_ref, f_ref, v_ref, floor_ref, extra_ref, gain_ref, aq_ref, lat_ref, rk_ref,
    lgain_ref, wup_ref, cos_ref, sin_ref, turn_ref, place_ref, swap_ref,
    lbuf, ssend, srecv, wbuf, psend, precv, out_ref, logw_ref,
    kbuf, vbuf, intra, qf_ref, qb_ref, sf_ref, sb_ref, act, whole_state, whole_decay,
    in_sem, own_sem, l_send, l_recv, f_send, f_recv, s_send, s_recv, w_send, w_recv, z_send,
    x_send, x_recv, o_sem,
):
    n_fs, span = sizes
    tokens, width = q_ref.shape
    heads = width // HG_DK
    att_heads = aq_ref.shape[1] // HEAD
    up = att_heads * (NOPE + VDIM)
    blocks = tokens // BLOCK
    latent_width = lat_ref.shape[1]
    columns = w1_hbm.shape[1]
    cut_rows = w2_hbm.shape[0]
    cuts = w1_hbm.shape[0] // cut_rows + 1
    groups = columns // LANES
    rows = tokens // 2
    half_rope = ROPE // 2

    sp, fs, tp = lax.axis_index("sp"), lax.axis_index("fs"), lax.axis_index("tp")
    place = lax.rem(sp, span)
    base = sp - place
    parity = lax.rem(place, 2)
    has_left, has_right = place > 0, place < span - 1
    left = {"sp": base + jnp.maximum(place - 1, 0)}
    right = {"sp": base + jnp.minimum(place + 1, span - 1)}
    pair = {"sp": base + flip_bits(place, 1)}
    partner = {"tp": 1 - tp}
    mesh_id = pl.DeviceIdType.MESH

    def fs_peer(j):
        return {"fs": flip_bits(fs, j)}

    direct, steps, order = transfer_plan(n_fs, span, groups, cuts)

    def at_chunk(v):
        g, b = divmod(v, cuts)
        return g + parity * (groups - 1 - 2 * g), b + parity * (cuts - 1 - 2 * b)

    def chunk(j, v):
        g, b = at_chunk(v)
        return wbuf.at[j, g, pl.ds(pl.multiple_of(b * cut_rows, cut_rows), cut_rows), :]

    def chunk_sem(sems, j, v):
        g, b = at_chunk(v)
        return sems.at[j, g * cuts + b]

    def fetch(k, src, dst):
        return pltpu.make_async_copy(src, dst, in_sem.at[k])

    own = []
    for g in range(groups):
        cols = pl.ds(g * LANES, LANES)
        for k, (src, at) in enumerate(((w1_hbm, 0), (w2_hbm, w1_hbm.shape[0]))):
            own.append(pltpu.make_async_copy(
                src.at[:, cols], wbuf.at[0, g, pl.ds(at, src.shape[0]), :], own_sem.at[2 * g + k]))
    for c in own:
        c.start()
    my_tokens = pl.ds(pl.multiple_of(place * tokens, tokens), tokens)
    tp_up = pl.ds(pl.multiple_of(tp * up, LANES), up)
    early = [
        fetch(0, lat_hbm, lat_ref), fetch(1, rk_hbm, rk_ref), fetch(2, lgain_hbm, lgain_ref),
        fetch(3, turn_hbm.at[:, my_tokens], turn_ref),
    ]
    gates = [
        fetch(4, f_hbm, f_ref), fetch(5, q_hbm, q_ref), fetch(6, v_hbm, v_ref),
        fetch(7, floor_hbm, floor_ref), fetch(8, extra_hbm, extra_ref),
    ]
    late = [
        fetch(9, gain_hbm, gain_ref), fetch(10, aq_hbm, aq_ref), fetch(11, wup_hbm.at[:, tp_up], wup_ref),
        fetch(12, cos_hbm.at[my_tokens, :], cos_ref), fetch(13, sin_hbm.at[my_tokens, :], sin_ref),
        fetch(14, place_hbm, place_ref), fetch(15, swap_hbm, swap_ref),
    ]
    for c in early + gates + late:
        c.start()

    barrier = pltpu.get_barrier_semaphore()
    for j in direct:
        pl.semaphore_signal(barrier, inc=1, device_id=fs_peer(j), device_id_type=mesh_id)
    pl.semaphore_signal(barrier, inc=1, device_id=partner, device_id_type=mesh_id)

    @pl.when(has_left)
    def _():
        pl.semaphore_signal(barrier, inc=1, device_id=left, device_id_type=mesh_id)

    @pl.when(has_right)
    def _():
        pl.semaphore_signal(barrier, inc=1, device_id=right, device_id_type=mesh_id)

    for c in own:
        c.wait()
    pl.semaphore_wait(barrier, len(direct) + 1 + has_left.astype(jnp.int32) + has_right.astype(jnp.int32))

    def remote(src, dst, send, recv, device):
        return pltpu.make_async_remote_copy(
            src_ref=src, dst_ref=dst, send_sem=send, recv_sem=recv,
            device_id=device, device_id_type=mesh_id,
        )

    sent = []

    def send(c):
        c.start()
        sent.append(c)

    for k in range(max((len(direct[j]) for j in direct), default=0)):
        for j in direct:
            if k < len(direct[j]):
                v = direct[j][k]
                send(remote(chunk(0, v), chunk(j, v), chunk_sem(w_send, j, v), chunk_sem(w_recv, j, v), fs_peer(j)))

    arrived = set()

    def await_chunk(j, v):
        if (j, v) not in arrived:
            arrived.add((j, v))
            remote(chunk(j, v), chunk(j, v), chunk_sem(w_send, j, v), chunk_sem(w_recv, j, v), fs_peer(j)).wait_recv()

    def relay_step(k):
        if k >= len(steps):
            return
        for (j, v), kind in steps[k]:
            await_chunk(j, v)
            if kind == "cross":
                send(remote(chunk(j, v), chunk(3, v), chunk_sem(w_send, 3, v), chunk_sem(w_recv, 3, v), fs_peer(3 - j)))
            else:
                send(remote(chunk(j, v), chunk(j, v), chunk_sem(z_send, j, v), chunk_sem(w_recv, j, v), pair))

    for c in early:
        c.wait()
    lat = lat_ref[...].astype(F32)
    normed = lat * lax.rsqrt(jnp.mean(lat * lat, axis=-1, keepdims=True) + norm_eps) * lgain_ref[...]
    normed = normed.astype(BF16)
    rope_a, rope_b = rk_ref[:half_rope, :].astype(F32), rk_ref[half_rope:, :].astype(F32)
    turn_c, turn_s = turn_ref[:half_rope, :], turn_ref[half_rope:, :]
    turned_a = (rope_a * turn_c - rope_b * turn_s).astype(BF16)
    turned_b = (rope_a * turn_s + rope_b * turn_c).astype(BF16)
    for t in range(2):
        part = slice(t * rows, (t + 1) * rows)
        lbuf[place, t, :rows, :] = normed[part]
        lbuf[place, t, rows:, :rows] = turned_a[:, part]
        lbuf[place, t, rows:, rows:] = turned_b[:, part]

    def along(d, at):
        return remote(lbuf.at[at, tp], lbuf.at[at, tp], l_send.at[d, at], l_recv.at[at], right if d == 0 else left)

    def across(at):
        return remote(lbuf.at[at, tp], lbuf.at[at, tp], f_send.at[at], f_recv.at[at], partner)

    @pl.when(has_right)
    def _():
        along(0, place).start()

    @pl.when(has_left)
    def _():
        along(1, place).start()

    def latent_round(r):
        for d in range(2):
            at = place - r if d == 0 else place + r
            there = at >= 0 if d == 0 else at < span
            at = jnp.clip(at, 0, span - 1)

            @pl.when(there)
            def _():
                along(d, at).wait_recv()
                across(at).start()

            if r < span - 1:
                @pl.when(jnp.logical_and(there, has_right if d == 0 else has_left))
                def _():
                    along(d, at).start()

    row = lax.broadcasted_iota(jnp.int32, (BLOCK, BLOCK), 0)
    col = lax.broadcasted_iota(jnp.int32, (BLOCK, BLOCK), 1)
    lower = row >= col
    upper = row <= col
    tri = (jnp.where(lower, 1.0, 0.0).astype(BF16), jnp.where(upper, 1.0, 0.0).astype(BF16))
    for c in gates:
        c.wait()
    spikes = lax.dot_general(
        extra_ref[...],
        jnp.where(
            lax.broadcasted_iota(jnp.int32, (heads, width), 0)
            == lax.broadcasted_iota(jnp.int32, (heads, width), 1) // HG_DK, 1.0, 0.0),
        (((0,), (0,)), ((), ())), precision=lax.Precision.HIGHEST, preferred_element_type=F32)
    block_decay = [[[None] * blocks for _ in range(2)] for _ in range(heads)]
    for h in range(heads):
        lanes = slice(h * HG_DK, (h + 1) * HG_DK)
        for b in range(blocks):
            tok = slice(b * BLOCK, (b + 1) * BLOCK)
            q = q_ref[tok, lanes].astype(F32)
            gate = f_ref[tok, lanes].astype(F32)
            v = v_ref[tok, lanes]
            miss = 1.0 / (1.0 + jnp.exp(gate))
            spike = spikes[tok, lanes]
            scores = None
            for d in range(2):
                keyed = (1.0 - floor_ref[d : d + 1, lanes]) * miss
                decay = jnp.log1p(-keyed) + spike
                hi = decay.astype(BF16)
                lo = (decay - hi.astype(F32)).astype(BF16)
                run = mm(tri[d], hi) + mm(tri[d], lo)
                mid_at = BLOCK // 2 - 1 if d == 0 else BLOCK // 2
                end_at = BLOCK - 1 if d == 0 else 0
                mid = run[mid_at : mid_at + 1]
                end = run[end_at : end_at + 1]
                grow = jnp.exp(run - mid)
                qd = q * grow
                kd = keyed * jnp.exp(mid - run)
                s = mm_nt(qd.astype(BF16), kd.astype(BF16))
                s = jnp.where(lower if d == 0 else upper, s, 0.0)
                scores = s if scores is None else scores + s
                cross = qf_ref if d == 0 else qb_ref
                cross[tok, lanes] = (qd * jnp.exp(mid)).astype(BF16)
                state = mm_tn(v, (kd * jnp.exp(end - mid)).astype(BF16))
                keep = sf_ref if d == 0 else sb_ref
                keep[b, :, lanes] = state
                block_decay[h][d][b] = jnp.exp(end)
            intra[tok, lanes] = mm(scores.astype(BF16), v)
        for d in range(2):
            keep = sf_ref if d == 0 else sb_ref
            going = range(blocks) if d == 0 else range(blocks - 1, -1, -1)
            total, decay_all = None, None
            for b in going:
                one = keep[b, :, lanes]
                dec = block_decay[h][d][b]
                total = one if total is None else total * dec + one
                decay_all = dec if decay_all is None else decay_all * dec
            whole_state[d, h] = total
            whole_decay[d, h] = jnp.broadcast_to(decay_all, (8, HG_DK))

    first = jnp.where(2 * place < span, 0, 1)

    def link(d, h):
        towards = jnp.clip(place + 1 - 2 * d, 0, span - 1)
        return remote(ssend.at[d, h], srecv.at[d, h], s_send.at[d, h], s_recv.at[d, h],
                      {"sp": base + towards})

    def has_previous(d):
        return jnp.where(d == 0, place, span - 1 - place) > 0

    def has_next(d):
        return jnp.where(d == 0, span - 1 - place, place) > 0

    def pass_on(d):
        for h in range(heads):
            @pl.when(has_previous(d))
            def _():
                link(d, h).wait_recv()

            @pl.when(jnp.logical_not(has_previous(d)))
            def _():
                srecv[d, h] = jnp.zeros((HG_DK, HG_DK), BF16)

            @pl.when(has_next(d))
            def _():
                reached = srecv[d, h].astype(F32) * whole_decay[d, h, 0:1] + whole_state[d, h]
                ssend[d, h] = reached.astype(BF16)
                link(d, h).start()

    @pl.when(jnp.logical_not(has_previous(first)))
    def _():
        pass_on(first)

    if span > 1:
        latent_round(1)
    relay_step(0)
    relay_step(1)

    @pl.when(has_previous(first))
    def _():
        pass_on(first)

    for r in range(2, span):
        latent_round(r)
        if r == 2:
            relay_step(2)

    @pl.when(has_next(1 - first))
    def _():
        pass_on(1 - first)

    for k in range(2, len(steps) - 2):
        if k > 2 or span < 3:
            relay_step(k)

    for c in late:
        c.wait()
    wup = wup_ref[...]
    lane = lax.broadcasted_iota(jnp.int32, (rows, LANES), 1)
    put_a = place_ref[NOPE : NOPE + half_rope, :LANES]
    put_b = place_ref[NOPE + half_rope : HEAD, :LANES]
    for j in range(span):
        at = flip_bits(place, j)
        if j > 0:
            across(at).wait_recv()
        for t in range(2):
            keys = slice((2 * j + t) * rows, (2 * j + t + 1) * rows)
            expanded = mm(lbuf[at, t, :rows, :], wup)
            rot = mm_tn(lbuf[at, t, rows:, :rows], put_a) + mm_tn(lbuf[at, t, rows:, rows:], put_b)
            vbuf[keys, :] = expanded.astype(BF16)
            for h in range(att_heads):
                lanes = slice(h * LANES, (h + 1) * LANES)
                kbuf[keys, lanes] = jnp.where(lane < NOPE, expanded[:, lanes], rot).astype(BF16)

    def act_slot(t):
        return t + tp * (1 - 2 * t)

    aq = aq_ref[...]
    cos, sin = cos_ref[...], sin_ref[...]
    scale = HEAD ** (-0.5)
    lane = lax.broadcasted_iota(jnp.int32, (tokens, LANES), 1)
    logw = jnp.zeros((tokens, LANES), F32)
    kept = None
    left_steps = list(range(max(len(steps) - 2, 2), len(steps)))
    for h in range(att_heads):
        lanes = slice(h * LANES, (h + 1) * LANES)
        query = mm(aq, place_ref[:, lanes]) * cos + mm(aq, swap_ref[:, lanes]) * sin
        scores = mm_nt(query.astype(BF16), kbuf[:, lanes]) * scale
        peak = jnp.max(scores, axis=-1, keepdims=True)
        weights = jnp.exp(scores - peak)
        totals = jnp.sum(weights, axis=-1, keepdims=True)
        result = mm(weights.astype(BF16), vbuf[:, lanes]) / totals
        logw = jnp.where(lane == h, peak + jnp.log(totals), logw)
        if h % 2 == 0:
            kept = pltpu.roll(result, VDIM, 1)
        else:
            at = width + (h // 2) * LANES
            joined = jnp.where(lane < VDIM, kept, result).astype(BF16)
            for t in range(2):
                act[act_slot(t), :, at : at + LANES] = joined[t * rows : (t + 1) * rows]
            if left_steps:
                relay_step(left_steps.pop(0))
    for k in left_steps:
        relay_step(k)
    logw_ref[...] = jnp.transpose(logw)[:att_heads]
    logw_copy = pltpu.make_async_copy(logw_ref, logw_hbm, o_sem.at[n_fs * groups])
    logw_copy.start()

    @pl.when(jnp.logical_not(has_next(1 - first)))
    def _():
        pass_on(1 - first)

    for h in range(heads):
        lanes = slice(h * HG_DK, (h + 1) * HG_DK)
        carry_f = srecv[0, h].astype(F32)
        carry_b = srecv[1, h].astype(F32)
        starts_f = []
        for b in range(blocks):
            starts_f.append(carry_f)
            carry_f = carry_f * block_decay[h][0][b] + sf_ref[b, :, lanes]
        starts_b = [None] * blocks
        for b in range(blocks - 1, -1, -1):
            starts_b[b] = carry_b
            carry_b = carry_b * block_decay[h][1][b] + sb_ref[b, :, lanes]
        for b in range(blocks):
            tok = slice(b * BLOCK, (b + 1) * BLOCK)
            t, off = divmod(b * BLOCK, rows)
            o = intra[tok, lanes]
            o = o + mm_nt(qf_ref[tok, lanes], starts_f[b].astype(BF16))
            o = o + mm_nt(qb_ref[tok, lanes], starts_b[b].astype(BF16))
            o = o * lax.rsqrt(jnp.mean(o * o, axis=-1, keepdims=True) + norm_eps) * gain_ref[:, lanes]
            act[act_slot(t), off : off + BLOCK, lanes] = o.astype(BF16)

    x_copies, out_copies = [], []

    def finish(i):
        j, g = order[i]
        x_copies[i].wait_recv()
        out_ref[i] = (out_ref[i].astype(F32) + precv[i].astype(F32)).astype(BF16)
        at = flip_bits(fs, j) * columns + (g + parity * (groups - 1 - 2 * g)) * LANES
        c = pltpu.make_async_copy(out_ref.at[i], out_hbm.at[:, pl.ds(pl.multiple_of(at, LANES), LANES)], o_sem.at[i])
        c.start()
        out_copies.append(c)

    behind = 2
    for i, (j, g) in enumerate(order):
        if j > 0:
            for b in range(cuts):
                await_chunk(j, g * cuts + b)
        weight = wbuf[j, g + parity * (groups - 1 - 2 * g)]
        away = mm(act[1], weight)
        psend[i] = away.astype(BF16)
        c = remote(psend.at[i], precv.at[i], x_send.at[i], x_recv.at[i], partner)
        c.start()
        x_copies.append(c)
        out_ref[i] = mm(act[0], weight).astype(BF16)
        if i >= behind:
            finish(i - behind)
    for i in range(max(len(order) - behind, 0), len(order)):
        finish(i)

    for c in sent + x_copies:
        c.wait_send()

    @pl.when(has_right)
    def _():
        along(0, place).wait_send()

    @pl.when(has_left)
    def _():
        along(1, place).wait_send()

    for r in range(1, span):
        for d in range(2):
            at = place - r if d == 0 else place + r
            there = at >= 0 if d == 0 else at < span
            at = jnp.clip(at, 0, span - 1)

            @pl.when(there)
            def _():
                across(at).wait_send()

            if r < span - 1:
                @pl.when(jnp.logical_and(there, has_right if d == 0 else has_left))
                def _():
                    along(d, at).wait_send()

    for d in range(2):
        for h in range(heads):
            @pl.when(has_next(d))
            def _():
                link(d, h).wait_send()

    for c in out_copies + [logw_copy]:
        c.wait()


def local(
    n_fs,
    n_sp,
    recurrent_query,
    forget_logits,
    recurrent_value,
    forget_floor,
    extra_log_decay,
    recurrent_norm_gain,
    attention_query,
    latent,
    rotary_key,
    latent_norm_gain,
    latent_up_weight,
    recurrent_output_weight,
    attention_output_weight,
):
    span = min(n_sp, widest_span)
    tokens, width = recurrent_query.shape[1:]
    heads = width // HG_DK
    att_heads = attention_query.shape[2] // HEAD
    latent_width = latent.shape[2]
    columns = recurrent_output_weight.shape[1]
    att_width = attention_output_weight.shape[0]
    up = att_heads * (NOPE + VDIM)
    blocks = tokens // BLOCK
    rows = tokens // 2
    groups = columns // LANES
    pieces = groups * n_fs
    chunks = groups * (width // att_width + 1)
    cos_pad, sin_pad, turns, place, swap = rope_constants(span * tokens, att_heads)
    anywhere = pl.BlockSpec(memory_space=pl.ANY)
    dma = pltpu.SemaphoreType.DMA
    vmem = pltpu.VMEM
    mixed, log_weight = pl.pallas_call(
        functools.partial(kernel, (n_fs, span)),
        out_shape=(
            jax.ShapeDtypeStruct((rows, columns * n_fs), BF16),
            jax.ShapeDtypeStruct((att_heads, tokens), F32),
        ),
        in_specs=[anywhere] * 18,
        out_specs=(anywhere, anywhere),
        scratch_shapes=[
            vmem((tokens, width), BF16), vmem((tokens, width), BF16), vmem((tokens, width), BF16),
            vmem((2, width), F32), vmem((heads, tokens), F32), vmem((1, width), F32),
            vmem((tokens, att_heads * HEAD), BF16), vmem((tokens, latent_width), BF16), vmem((ROPE, tokens), BF16),
            vmem((1, latent_width), F32), vmem((latent_width, up), BF16),
            vmem((tokens, LANES), F32), vmem((tokens, LANES), F32), vmem((ROPE, tokens), F32),
            vmem((att_heads * HEAD, att_heads * LANES), BF16), vmem((att_heads * HEAD, att_heads * LANES), BF16),
            vmem((span, 2, rows + ROPE // 2, latent_width), BF16),
            vmem((2, heads, HG_DK, HG_DK), BF16),
            vmem((2, heads, HG_DK, HG_DK), BF16),
            vmem((n_fs, groups, width + att_width, LANES), BF16),
            vmem((pieces, rows, LANES), BF16),
            vmem((pieces, rows, LANES), BF16),
            vmem((pieces, rows, LANES), BF16),
            vmem((att_heads, tokens), F32),
            vmem((span * tokens, att_heads * LANES), BF16),
            vmem((span * tokens, att_heads * LANES), BF16),
            vmem((tokens, width), F32),
            vmem((tokens, width), BF16),
            vmem((tokens, width), BF16),
            vmem((blocks, HG_DK, width), F32),
            vmem((blocks, HG_DK, width), F32),
            vmem((2, rows, width + att_width), BF16),
            vmem((2, heads, HG_DK, HG_DK), F32),
            vmem((2, heads, 8, HG_DK), F32),
            dma((16,)), dma((2 * groups,)), dma((2, span)), dma((span,)), dma((span,)), dma((span,)),
            dma((2, heads)), dma((2, heads)),
            dma((n_fs, chunks)), dma((n_fs, chunks)), dma((n_fs, chunks)),
            dma((pieces,)), dma((pieces,)), dma((pieces + 1,)),
        ],
        compiler_params=pltpu.CompilerParams(
            collective_id=0, has_side_effects=True, vmem_limit_bytes=56 * 2**20
        ),
        name="mixers",
    )(
        recurrent_query[0],
        forget_logits[0],
        recurrent_value[0],
        forget_floor,
        extra_log_decay[0].T,
        recurrent_norm_gain[None],
        attention_query[0],
        latent[0],
        rotary_key[0].T,
        latent_norm_gain[None],
        latent_up_weight,
        jnp.asarray(cos_pad),
        jnp.asarray(sin_pad),
        jnp.asarray(turns),
        jnp.asarray(place, BF16),
        jnp.asarray(swap, BF16),
        recurrent_output_weight,
        attention_output_weight,
    )
    return mixed[None], log_weight.T[None]


def solution(mesh):
    placed = (
        P("fs", "sp", "tp"),
        P("fs", "sp", "tp"),
        P("fs", "sp", "tp"),
        P(None, "tp"),
        P("fs", "sp", "tp"),
        P("tp"),
        P("fs", "sp", "tp"),
        P("fs", "sp", None),
        P("fs", "sp", None),
        P(),
        P(),
        P("tp", "fs"),
        P("tp", "fs"),
    )
    return jax.shard_map(
        functools.partial(local, mesh.shape["fs"], mesh.shape["sp"]),
        mesh=mesh,
        in_specs=placed,
        out_specs=(P("fs", ("sp", "tp"), None), P("fs", "sp", "tp")),
        check_vma=False,
    )
```

time: 42.1 us -> 39.1 us (0.929)
  Pallas kernels: 38.8 us -> 35.8 us
    pallas_call x1, Pallas kernels: 38.8 us -> 35.8 us  [local(): pl.pallas_call(functools.partial(kernel, (n_fs, span)), out_shape=(jax.Sh...]
where the time goes in v1:
time: 39.1 us; the launch traced here: 39 us
  Pallas kernels  35.8 us (92%)
  local copies, waits for them, and re-layouts  2.48 us (6%)
  between operations  0.65 us (2%)
    pallas_call x1, Pallas kernels, local(): pl.pallas_call(functools.partial(kernel, (n_fs, span)), out_shape=(jax.Sh...  35.8 us
    unnamed x4, local copies, waits for them, and re-layouts  2.48 us

profile of v1, /device:TPU:0, one launch (start us, length us, event | category | flops | bytes accessed | tf_op | source)
XLA Modules:
  0.0 39.0 jit_solution(18157853882866084885)
XLA Ops:
  0.6 35.8 %mixers.1 = (bf16[128,2048]{1,0:T(8,128)(2,1)}, f32[4,256]{1,0:T(4,128)}) custom-call(bf16[256,512]{1,0:T(8,128)(2,1)} %bitcast.18, bf16[256,512]{1,0:T(8,128)(2,1)} %bitcast.19, bf16[256,512]{1,0:T(8,128)(2,1)} %bitcast.20, f32[2,512]{1,0:T(2,128)} %floor_hbm.1, f32[4,256]{1,0:T(4,128)} %bitcast.24, f32[1,512]{1,0:T(1,128)} %bitcast.26, ...), custom_call_target="tpu_custom_call" | custom-call | tf_op jit(solution)/shard_map/mixers/pallas_call | solution.py:573
  36.5 0.0 copy-start
  36.5 1.9 %copy.22 = bf16[1,128,2048]{2,1,0:T(8,128)(2,1)} copy(bf16[1,128,2048]{2,1,0:T(8,128)(2,1)} %bitcast.17) | data formatting | bytes 1048576
  38.4 0.0 copy-done
  38.4 0.6 %copy.23 = f32[1,256,4]{1,2,0:T(4,128)} copy(f32[1,256,4]{1,2,0:T(4,128)S(1)} %bitcast.25) | data formatting | bytes 8192
Async XLA Ops:
  36.5 1.9 %copy-start = (f32[4,256]{1,0:T(4,128)S(1)}, f32[4,256]{1,0:T(4,128)}, u32[]{:S(2)}) copy-start(f32[4,256]{1,0:T(4,128)} %get-tuple-element.5) | copy-start | bytes 12292

commit v2 on v1

v2 whole, which is shorter than its diff:
```python
import functools

import jax
import jax.numpy as jnp
import numpy as np
from jax import lax
from jax.experimental import pallas as pl
from jax.experimental.pallas import tpu as pltpu
from jax.sharding import PartitionSpec as P

HG_DK = 128
NOPE = 64
ROPE = 32
VDIM = 64
HEAD = NOPE + ROPE
LANES = 128
BLOCK = 128

norm_eps = 1e-06
rope_base = 10000.0
widest_span = 8

F32 = jnp.float32
BF16 = jnp.bfloat16


def mm(a, b):
    return jnp.dot(a, b, preferred_element_type=F32)


def mm_nt(a, b):
    return lax.dot_general(a, b, (((1,), (1,)), ((), ())), preferred_element_type=F32)


def mm_tn(a, b):
    return lax.dot_general(a, b, (((0,), (0,)), ((), ())), preferred_element_type=F32)


def flip_bits(value, mask):
    bit = 1
    while bit <= mask:
        if mask & bit:
            value = value + bit - 2 * bit * lax.rem(value // bit, 2)
        bit *= 2
    return value


def window_start(h, heads):
    return min(h * HEAD // LANES * LANES, max(heads * HEAD - 2 * LANES, 0))


def rope_constants(seq_len, heads):
    half = ROPE // 2
    inverse = (np.float32(rope_base) ** (-np.arange(half, dtype=np.float32) / np.float32(half))).astype(np.float32)
    angles = np.arange(seq_len, dtype=np.float32)[:, None] * inverse[None, :]
    cos_pad = np.zeros((seq_len, LANES), np.float32)
    sin_pad = np.zeros((seq_len, LANES), np.float32)
    cos_pad[:, :NOPE] = 1.0
    cos_pad[:, NOPE:HEAD] = np.tile(np.cos(angles), (1, 2))
    sin_pad[:, NOPE:HEAD] = np.tile(np.sin(angles), (1, 2))
    turns = np.concatenate([np.cos(angles).T, np.sin(angles).T], axis=0)
    window = min(2 * LANES, heads * HEAD)
    spread = np.zeros((heads, window, 2 * LANES), np.float32)
    for h in range(heads):
        off = h * HEAD - window_start(h, heads)
        for i in range(HEAD):
            spread[h, off + i, i] = 1.0
        for i in range(half):
            a, b = NOPE + i, NOPE + half + i
            spread[h, off + b, LANES + a] = -1.0
            spread[h, off + a, LANES + b] = 1.0
    return cos_pad, sin_pad, turns, spread


def transfer_plan(n_fs, span, groups, cuts):
    count = groups * cuts
    paired = span % 2 == 0
    if n_fs == 4 and paired:
        direct = count - count // 3
        lists = {1: list(range(direct)), 2: list(range(count - 1, count - 1 - direct, -1))}
        half = count // 2
        cross = [(1, v) for v in range(half)], [(2, v) for v in range(count - 1, half - 1, -1)]
        over = [(1, v) for v in range(count - direct)], [(2, v) for v in range(count - 1, direct - 1, -1)]
        crosses = [[c[k] for c in cross] for k in range(half)]
        pairs = [c[k] for k in range(count - direct) for c in over]
        when = {}
        for k in range(direct):
            when[1, lists[1][k]] = when[2, lists[2][k]] = k + 1
        for k in range(half):
            when[3, cross[0][k][1]] = when[3, cross[1][k][1]] = direct + k + 1
        for k in range(count - direct):
            when[1, count - 1 - over[0][k][1]] = 5 + 2 * k
            when[2, count - 1 - over[1][k][1]] = 6 + 2 * k
    else:
        lists = {j: list(range(count)) for j in range(1, n_fs)}
        crosses, pairs = [], []
        when = {(j, v): v * n_fs + j for j in lists for v in lists[j]}
    last = {(j, g): max(when[j, g * cuts + b] for b in range(cuts)) for j in range(1, n_fs) for g in range(groups)}
    order = [(0, g) for g in range(groups)] + sorted(last, key=lambda one: (last[one], one))
    bounds = [0, len(order) // 2, 3 * len(order) // 4, len(order)]
    batches = []
    for lo, hi in zip(bounds, bounds[1:]):
        batch = []
        for j, g in sorted(order[lo:hi]):
            if batch and batch[-1][0] == j and batch[-1][1] + batch[-1][2] == g and batch[-1][2] == 1:
                batch[-1] = (j, batch[-1][1], 2)
            else:
                batch.append((j, g, 1))
        batches.append(batch)
    return lists, crosses, pairs, batches


def kernel(
    sizes,
    q_hbm, f_hbm, v_hbm, floor_hbm, extra_hbm, gain_hbm, aq_hbm, lat_hbm, rk_hbm,
    lgain_hbm, wup_hbm, cos_hbm, sin_hbm, turn_hbm, spread_hbm, w1_hbm, w2_hbm,
    out_ref, logw_ref,
    q_ref, f_ref, v_ref, floor_ref, extra_ref, gain_ref, aq_ref, lat_ref, rk_ref,
    lgain_ref, wup_ref, cos_ref, sin_ref, turn_ref, spread_ref,
    lbuf, ssend, srecv, wbuf, psend, precv, keep,
    kbuf, vbuf, intra, qd_ref, kd_ref, qc_ref, st_ref, act, whole_state, whole_decay,
    in_sem, own_sem, l_send, l_recv, f_send, f_recv, s_send, s_recv, w_send, w_recv,
    x_send, x_recv,
):
    n_fs, span = sizes
    tokens, width = q_ref.shape
    heads = width // HG_DK
    att_heads = aq_ref.shape[1] // HEAD
    up = att_heads * (NOPE + VDIM)
    blocks = tokens // BLOCK
    latent_width = lat_ref.shape[1]
    columns = w1_hbm.shape[1]
    cut_rows = w2_hbm.shape[0]
    cuts = w1_hbm.shape[0] // cut_rows + 1
    groups = columns // LANES
    rows = tokens // 2
    half_rope = ROPE // 2

    sp, fs, tp = lax.axis_index("sp"), lax.axis_index("fs"), lax.axis_index("tp")
    place = lax.rem(sp, span)
    base = sp - place
    parity = lax.rem(place, 2)
    has_left, has_right = place > 0, place < span - 1
    left = {"sp": base + jnp.maximum(place - 1, 0)}
    right = {"sp": base + jnp.minimum(place + 1, span - 1)}
    pair = {"sp": base + flip_bits(place, 1)}
    partner = {"tp": 1 - tp}
    mesh_id = pl.DeviceIdType.MESH

    def fs_peer(j):
        return {"fs": flip_bits(fs, j)}

    direct, crosses, pairs, batches = transfer_plan(n_fs, span, groups, cuts)

    def at_chunk(v):
        g, b = divmod(v, cuts)
        return g + parity * (groups - 1 - 2 * g), b + parity * (cuts - 1 - 2 * b)

    def chunk(j, v):
        g, b = at_chunk(v)
        return wbuf.at[j, pl.ds(pl.multiple_of(b * cut_rows, cut_rows), cut_rows),
                       pl.ds(pl.multiple_of(g * LANES, LANES), LANES)]

    relayed = set(pairs).union(*crosses)

    def alone(j, v):
        return any((j, v - v % cuts + b) in relayed for b in range(cuts))

    def arrival(j, v, seen):
        g, b = at_chunk(v)
        return w_recv.at[j - 1, g * cuts + (b if alone(j, seen) else 0)]

    def remote(src, dst, send, recv, device):
        return pltpu.make_async_remote_copy(
            src_ref=src, dst_ref=dst, send_sem=send, recv_sem=recv,
            device_id=device, device_id_type=mesh_id,
        )

    def fetch(k, src, dst):
        return pltpu.make_async_copy(src, dst, in_sem.at[k])

    own = [
        pltpu.make_async_copy(src, wbuf.at[0, pl.ds(at, src.shape[0]), :], own_sem.at[k])
        for k, (src, at) in enumerate(((w1_hbm, 0), (w2_hbm, w1_hbm.shape[0])))
    ]
    for c in own:
        c.start()
    my_tokens = pl.ds(pl.multiple_of(place * tokens, tokens), tokens)
    tp_up = pl.ds(pl.multiple_of(tp * up, LANES), up)
    early = [
        fetch(0, lat_hbm, lat_ref), fetch(1, rk_hbm, rk_ref), fetch(2, lgain_hbm, lgain_ref),
        fetch(3, turn_hbm.at[:, my_tokens], turn_ref),
    ]
    gates = [
        fetch(4, f_hbm, f_ref), fetch(5, q_hbm, q_ref), fetch(6, v_hbm, v_ref),
        fetch(7, floor_hbm, floor_ref), fetch(8, extra_hbm, extra_ref),
    ]
    late = [
        fetch(9, gain_hbm, gain_ref), fetch(10, aq_hbm, aq_ref), fetch(11, wup_hbm.at[:, tp_up], wup_ref),
        fetch(12, cos_hbm.at[my_tokens, :], cos_ref), fetch(13, sin_hbm.at[my_tokens, :], sin_ref),
        fetch(14, spread_hbm, spread_ref),
    ]
    for c in early + gates + late:
        c.start()

    barrier = pltpu.get_barrier_semaphore()
    for j in direct:
        pl.semaphore_signal(barrier, inc=1, device_id=fs_peer(j), device_id_type=mesh_id)
    pl.semaphore_signal(barrier, inc=1, device_id=partner, device_id_type=mesh_id)

    @pl.when(has_left)
    def _():
        pl.semaphore_signal(barrier, inc=1, device_id=left, device_id_type=mesh_id)

    @pl.when(has_right)
    def _():
        pl.semaphore_signal(barrier, inc=1, device_id=right, device_id_type=mesh_id)

    for c in early:
        c.wait()
    lat = lat_ref[...].astype(F32)
    normed = lat * lax.rsqrt(jnp.mean(lat * lat, axis=-1, keepdims=True) + norm_eps) * lgain_ref[...]
    normed = normed.astype(BF16)
    rope_a, rope_b = rk_ref[:half_rope, :].astype(F32), rk_ref[half_rope:, :].astype(F32)
    turn_c, turn_s = turn_ref[:half_rope, :], turn_ref[half_rope:, :]
    turned_a = (rope_a * turn_c - rope_b * turn_s).astype(BF16)
    turned_b = (rope_a * turn_s + rope_b * turn_c).astype(BF16)
    for t in range(2):
        part = slice(t * rows, (t + 1) * rows)
        lbuf[place, t, :rows, :] = normed[part]
        lbuf[place, t, rows:, :rows] = turned_a[:, part]
        lbuf[place, t, rows:, rows:] = turned_b[:, part]

    def source(d, r):
        at = place - r if d == 0 else place + r
        there = at >= 0 if d == 0 else at < span
        onward = jnp.logical_and(there, has_right if d == 0 else has_left)
        return jnp.clip(at, 0, span - 1), there, onward

    def along(d, at):
        return remote(lbuf.at[at, tp], lbuf.at[at, tp], l_send.at[d, at], l_recv.at[at], right if d == 0 else left)

    def across(at):
        return remote(lbuf.at[at, tp], lbuf.at[at, tp], f_send.at[at], f_recv.at[at], partner)

    def latent_round(r):
        for d in range(2):
            at, there, onward = source(d, r)
            if r > 0:
                @pl.when(there)
                def _():
                    along(d, at).wait_recv()
                    across(at).start()

            if r < span - 1:
                @pl.when(onward)
                def _():
                    along(d, at).start()

    for c in own:
        c.wait()
    pl.semaphore_wait(barrier, len(direct) + 1 + has_left.astype(jnp.int32) + has_right.astype(jnp.int32))
    latent_round(0)
    for k in range(max((len(direct[j]) for j in direct), default=0)):
        for j in direct:
            if k < len(direct[j]):
                v = direct[j][k]
                remote(chunk(0, v), chunk(j, v), w_send.at[0], arrival(j, v, v), fs_peer(j)).start()
    arrived = set()

    def await_chunk(j, v):
        if not alone(j, v):
            v -= v % cuts
        if (j, v) in arrived:
            return
        arrived.add((j, v))
        ref = chunk(j, v)
        if not alone(j, v):
            ref = wbuf.at[j, :, pl.ds(pl.multiple_of(at_chunk(v)[0] * LANES, LANES), LANES)]
        remote(ref, ref, w_send.at[0], arrival(j, v, v), partner).wait_recv()

    def relay_cross(*ks):
        for k in ks:
            for j, v in crosses[k] if k < len(crosses) else ():
                await_chunk(j, v)
                remote(chunk(j, v), chunk(3, v), w_send.at[0], arrival(3, v, v), fs_peer(3 - j)).start()

    def relay_pair(lo, hi):
        for j, v in pairs[lo:hi]:
            await_chunk(j, v)
            seen = groups * cuts - 1 - v
            remote(chunk(j, v), chunk(j, v), w_send.at[0], arrival(j, v, seen), pair).start()

    row = lax.broadcasted_iota(jnp.int32, (BLOCK, BLOCK), 0)
    col = lax.broadcasted_iota(jnp.int32, (BLOCK, BLOCK), 1)
    lower = row >= col
    upper = row <= col
    tri = (jnp.where(lower, 1.0, 0.0).astype(BF16), jnp.where(upper, 1.0, 0.0).astype(BF16))
    for c in gates:
        c.wait()
    spikes = lax.dot_general(
        extra_ref[...],
        jnp.where(
            lax.broadcasted_iota(jnp.int32, (heads, width), 0)
            == lax.broadcasted_iota(jnp.int32, (heads, width), 1) // HG_DK, 1.0, 0.0),
        (((0,), (0,)), ((), ())), precision=lax.Precision.HIGHEST, preferred_element_type=F32)
    first = jnp.where(2 * place < span, 0, 1)

    def link(d, h):
        towards = jnp.clip(place + 1 - 2 * d, 0, span - 1)
        return remote(ssend.at[d, h], srecv.at[d, h], s_send.at[d], s_recv.at[d, h],
                      {"sp": base + towards})

    def has_previous(d):
        return jnp.where(d == 0, place, span - 1 - place) > 0

    def has_next(d):
        return jnp.where(d == 0, span - 1 - place, place) > 0

    def pass_head(d, h):
        @pl.when(has_previous(d))
        def _():
            link(d, h).wait_recv()

        @pl.when(jnp.logical_not(has_previous(d)))
        def _():
            srecv[d, h] = jnp.zeros((HG_DK, HG_DK), BF16)

        @pl.when(has_next(d))
        def _():
            reached = srecv[d, h].astype(F32) * whole_decay[d, h, 0:1] + whole_state[d, h]
            ssend[d, h] = reached.astype(BF16)
            link(d, h).start()

    def pass_on(d):
        for h in range(heads):
            pass_head(d, h)

    twice = [jnp.concatenate([t, t], axis=1) for t in tri]
    block_decay = [[[None] * blocks for _ in range(2)] for _ in range(heads)]
    ahead = 2 if heads % 2 == 0 else 1
    for h0 in range(0, heads, ahead):
        wide_lanes = slice(h0 * HG_DK, (h0 + ahead) * HG_DK)
        for b in range(blocks):
            tok = slice(b * BLOCK, (b + 1) * BLOCK)
            q = q_ref[tok, wide_lanes].astype(F32)
            miss = 1.0 / (1.0 + jnp.exp(f_ref[tok, wide_lanes].astype(F32)))
            spike = spikes[tok, wide_lanes]
            ending = []
            for d in range(2):
                keyed = (1.0 - floor_ref[d : d + 1, wide_lanes]) * miss
                decay = jnp.log1p(-keyed) + spike
                hi = decay.astype(BF16)
                lo = (decay - hi.astype(F32)).astype(BF16)
                run = mm(twice[d], jnp.concatenate([hi, lo], axis=0))
                mid_at = BLOCK // 2 - 1 if d == 0 else BLOCK // 2
                end_at = BLOCK - 1 if d == 0 else 0
                mid = run[mid_at : mid_at + 1]
                end = run[end_at : end_at + 1]
                qd = q * jnp.exp(run - mid)
                kd = keyed * jnp.exp(mid - run)
                qd_ref[d, tok, wide_lanes] = qd.astype(BF16)
                kd_ref[d, tok, wide_lanes] = kd.astype(BF16)
                reach = (qd * jnp.exp(mid)).astype(BF16)
                ending.append((kd * jnp.exp(end - mid)).astype(BF16))
                last = jnp.exp(end)
                for i in range(ahead):
                    one = slice(i * HG_DK, (i + 1) * HG_DK)
                    qc_ref[tok, (2 * (h0 + i) + d) * HG_DK : (2 * (h0 + i) + d + 1) * HG_DK] = reach[:, one]
                    block_decay[h0 + i][d][b] = last[:, one]
            for i in range(ahead):
                h = h0 + i
                one = slice(i * HG_DK, (i + 1) * HG_DK)
                both = jnp.concatenate([e[:, one] for e in ending], axis=1)
                st_ref[b, h] = mm_tn(v_ref[tok, h * HG_DK : (h + 1) * HG_DK], both)
        for h in range(h0, h0 + ahead):
            for d in range(2):
                side = slice(d * HG_DK, (d + 1) * HG_DK)
                going = range(blocks) if d == 0 else range(blocks - 1, -1, -1)
                total, decay_all = None, None
                for b in going:
                    one = st_ref[b, h, :, side]
                    dec = block_decay[h][d][b]
                    total = one if total is None else total * dec + one
                    decay_all = dec if decay_all is None else decay_all * dec
                whole_state[d, h] = total
                whole_decay[d, h] = jnp.broadcast_to(decay_all, (8, HG_DK))

    if span > 1:
        latent_round(1)
    relay_pair(0, 2)

    @pl.when(jnp.logical_not(has_previous(first)))
    def _():
        pass_on(first)

    for h in range(heads):
        lanes = slice(h * HG_DK, (h + 1) * HG_DK)
        for b in range(blocks):
            tok = slice(b * BLOCK, (b + 1) * BLOCK)
            scores = None
            for d in range(2):
                s = mm_nt(qd_ref[d, tok, lanes], kd_ref[d, tok, lanes])
                s = jnp.where(lower if d == 0 else upper, s, 0.0)
                scores = s if scores is None else scores + s
            intra[tok, lanes] = mm(scores.astype(BF16), v_ref[tok, lanes])

    for c in late:
        c.wait()
    wup = wup_ref[...]
    half_lane = lax.broadcasted_iota(jnp.int32, (rows, LANES), 1)
    put_a = spread_ref[0, NOPE : NOPE + half_rope, :LANES]
    put_b = spread_ref[0, NOPE + half_rope : HEAD, :LANES]

    def expand(j):
        at = flip_bits(place, j)
        for t in range(2):
            keys = slice((2 * j + t) * rows, (2 * j + t + 1) * rows)
            expanded = mm(lbuf[at, t, :rows, :], wup)
            rot = mm_tn(lbuf[at, t, rows:, :rows], put_a) + mm_tn(lbuf[at, t, rows:, rows:], put_b)
            vbuf[keys, :] = expanded.astype(BF16)
            for h in range(att_heads):
                lanes = slice(h * LANES, (h + 1) * LANES)
                kbuf[keys, lanes] = jnp.where(half_lane < NOPE, expanded[:, lanes], rot).astype(BF16)

    for j in range(1, min(2, span)):
        across(flip_bits(place, j)).wait_recv()
    for j in range(min(2, span)):
        expand(j)
    relay_cross(0, 1)
    if span > 2:
        latent_round(2)
    relay_pair(2, 3)
    relay_cross(2)

    @pl.when(has_previous(first))
    def _():
        pass_on(first)

    relay_cross(3)
    for r in range(3, span):
        latent_round(r)
    for j in range(2, span):
        across(flip_bits(place, j)).wait_recv()
    for j in range(2, span):
        expand(j)
    relay_cross(4)

    def act_slot(t):
        return t + tp * (1 - 2 * t)

    cos, sin = cos_ref[...], sin_ref[...]
    scale = HEAD ** (-0.5)
    lane = lax.broadcasted_iota(jnp.int32, (tokens, LANES), 1)
    logw = jnp.zeros((tokens, LANES), F32)
    kept = None
    for h in range(att_heads):
        lanes = slice(h * LANES, (h + 1) * LANES)
        start = window_start(h, att_heads)
        placed = mm(aq_ref[:, start : start + spread_ref.shape[1]], spread_ref[h])
        query = placed[:, :LANES] * cos + placed[:, LANES:] * sin
        scores = mm_nt(query.astype(BF16), kbuf[:, lanes]) * scale
        peak = jnp.max(scores, axis=-1, keepdims=True)
        weights = jnp.exp(scores - peak)
        totals = jnp.sum(weights, axis=-1, keepdims=True)
        result = mm(weights.astype(BF16), vbuf[:, lanes]) / totals
        logw = jnp.where(lane == h, peak + jnp.log(totals), logw)
        if h % 2 == 0:
            kept = pltpu.roll(result, VDIM, 1)
        else:
            at = width + (h // 2) * LANES
            joined = jnp.where(lane < VDIM, kept, result).astype(BF16)
            for t in range(2):
                act[act_slot(t), :, at : at + LANES] = joined[t * rows : (t + 1) * rows]
            if h == 1:
                @pl.when(has_next(1 - first))
                def _():
                    pass_on(1 - first)

                relay_pair(3, len(pairs))
                relay_cross(5)
    relay_cross(*range(6, len(crosses)))
    logw_ref[...] = jnp.transpose(logw)[:att_heads]

    @pl.when(jnp.logical_not(has_next(1 - first)))
    def _():
        pass_on(1 - first)

    for h in range(heads):
        lanes = slice(h * HG_DK, (h + 1) * HG_DK)
        carry = [srecv[d, h].astype(F32) for d in range(2)]
        starts = [[None] * blocks for _ in range(2)]
        for d in range(2):
            side = slice(d * HG_DK, (d + 1) * HG_DK)
            for b in range(blocks) if d == 0 else range(blocks - 1, -1, -1):
                starts[d][b] = carry[d].astype(BF16)
                carry[d] = carry[d] * block_decay[h][d][b] + st_ref[b, h, :, side]
        for b in range(blocks):
            tok = slice(b * BLOCK, (b + 1) * BLOCK)
            t, off = divmod(b * BLOCK, rows)
            begin = jnp.concatenate([starts[0][b], starts[1][b]], axis=1)
            o = intra[tok, lanes] + mm_nt(qc_ref[tok, 2 * h * HG_DK : 2 * (h + 1) * HG_DK], begin)
            o = o * lax.rsqrt(jnp.mean(o * o, axis=-1, keepdims=True) + norm_eps) * gain_ref[:, lanes]
            act[act_slot(t), off : off + BLOCK, lanes] = o.astype(BF16)

    def real_at(g, n):
        return pl.multiple_of((g + parity * (groups - n - 2 * g)) * LANES, LANES)

    x_copies, spans = [], []
    top = act.shape[2]

    def finish(n):
        lo, hi = spans[n]
        x_copies[n].wait_recv()
        at = lo
        for j, g, many in batches[n]:
            w = many * LANES
            there = pl.multiple_of(flip_bits(fs, j) * columns + real_at(g, many), LANES)
            both = keep[:, at : at + w].astype(F32) + precv[:, at : at + w].astype(F32)
            out_ref[:, pl.ds(there, w)] = both.astype(BF16)
            at += w

    offset = 0
    for n, batch in enumerate(batches):
        for j, g, many in batch:
            if j > 0:
                for v in range(g * cuts, (g + many) * cuts):
                    await_chunk(j, v)
        start = offset
        for j, g, many in batch:
            w = many * LANES
            both = mm(act[...].reshape(2 * rows, top), wbuf[j, :, pl.ds(real_at(g, many), w)]).astype(BF16)
            psend[:, offset : offset + w] = both[rows:]
            keep[:, offset : offset + w] = both[:rows]
            offset += w
        part = slice(start, offset)
        spans.append((start, offset))
        c = remote(psend.at[:, part], precv.at[:, part], x_send.at[n], x_recv.at[n], partner)
        c.start()
        x_copies.append(c)
        if n > 0:
            finish(n - 1)
    finish(len(batches) - 1)

    if direct:
        remote(wbuf.at[1:], wbuf.at[1:], w_send.at[0], w_recv.at[0, 0], partner).wait_send()
    for c in x_copies:
        c.wait_send()

    for r in range(span):
        for d in range(2):
            at, there, onward = source(d, r)
            if r > 0:
                @pl.when(there)
                def _():
                    across(at).wait_send()

            if r < span - 1:
                @pl.when(onward)
                def _():
                    along(d, at).wait_send()

    for d in range(2):
        @pl.when(has_next(d))
        def _():
            remote(ssend.at[d], srecv.at[d], s_send.at[d], s_recv.at[d, 0], partner).wait_send()


def local(
    n_fs,
    n_sp,
    recurrent_query,
    forget_logits,
    recurrent_value,
    forget_floor,
    extra_log_decay,
    recurrent_norm_gain,
    attention_query,
    latent,
    rotary_key,
    latent_norm_gain,
    latent_up_weight,
    recurrent_output_weight,
    attention_output_weight,
):
    span = min(n_sp, widest_span)
    tokens, width = recurrent_query.shape[1:]
    heads = width // HG_DK
    att_heads = attention_query.shape[2] // HEAD
    latent_width = latent.shape[2]
    columns = recurrent_output_weight.shape[1]
    att_width = attention_output_weight.shape[0]
    up = att_heads * (NOPE + VDIM)
    blocks = tokens // BLOCK
    rows = tokens // 2
    groups = columns // LANES
    chunks = groups * (width // att_width + 1)
    cos_pad, sin_pad, turns, spread = rope_constants(span * tokens, att_heads)
    vmem = pltpu.VMEM
    whole = pl.BlockSpec(memory_space=vmem)
    hbm = pl.BlockSpec(memory_space=pltpu.HBM)
    dma = pltpu.SemaphoreType.DMA
    mixed, log_weight = pl.pallas_call(
        functools.partial(kernel, (n_fs, span)),
        out_shape=(
            vmem((rows, columns * n_fs), BF16),
            vmem((att_heads, tokens), F32),
        ),
        in_specs=[hbm] * 17,
        out_specs=(whole, whole),
        scratch_shapes=[
            vmem((tokens, width), BF16), vmem((tokens, width), BF16), vmem((tokens, width), BF16),
            vmem((2, width), F32), vmem((heads, tokens), F32), vmem((1, width), F32),
            vmem((tokens, att_heads * HEAD), BF16), vmem((tokens, latent_width), BF16), vmem((ROPE, tokens), BF16),
            vmem((1, latent_width), F32), vmem((latent_width, up), BF16),
            vmem((tokens, LANES), F32), vmem((tokens, LANES), F32), vmem((ROPE, tokens), F32),
            vmem(spread.shape, BF16),
            vmem((span, 2, rows + ROPE // 2, latent_width), BF16),
            vmem((2, heads, HG_DK, HG_DK), BF16),
            vmem((2, heads, HG_DK, HG_DK), BF16),
            vmem((n_fs, width + att_width, columns), BF16),
            vmem((rows, n_fs * columns), BF16),
            vmem((rows, n_fs * columns), BF16),
            vmem((rows, n_fs * columns), BF16),
            vmem((span * tokens, att_heads * LANES), BF16),
            vmem((span * tokens, att_heads * LANES), BF16),
            vmem((tokens, width), F32),
            vmem((2, tokens, width), BF16),
            vmem((2, tokens, width), BF16),
            vmem((tokens, 2 * width), BF16),
            vmem((blocks, heads, HG_DK, 2 * HG_DK), F32),
            vmem((2, rows, width + att_width), BF16),
            vmem((2, heads, HG_DK, HG_DK), F32),
            vmem((2, heads, 8, HG_DK), F32),
            dma((15,)), dma((2,)), dma((2, span)), dma((span,)), dma((span,)), dma((span,)),
            dma((2,)), dma((2, heads)),
            dma((1,)), dma((max(n_fs - 1, 1), chunks)),
            dma((3,)), dma((3,)),
        ],
        compiler_params=pltpu.CompilerParams(
            collective_id=0, has_side_effects=True, vmem_limit_bytes=56 * 2**20
        ),
        name="mixers",
    )(
        recurrent_query[0],
        forget_logits[0],
        recurrent_value[0],
        forget_floor,
        extra_log_decay[0].T,
        recurrent_norm_gain[None],
        attention_query[0],
        latent[0],
        rotary_key[0].T,
        latent_norm_gain[None],
        latent_up_weight,
        jnp.asarray(cos_pad),
        jnp.asarray(sin_pad),
        jnp.asarray(turns),
        jnp.asarray(spread, BF16),
        recurrent_output_weight,
        attention_output_weight,
    )
    return mixed[None], log_weight.T[None]


def solution(mesh):
    placed = (
        P("fs", "sp", "tp"),
        P("fs", "sp", "tp"),
        P("fs", "sp", "tp"),
        P(None, "tp"),
        P("fs", "sp", "tp"),
        P("tp"),
        P("fs", "sp", "tp"),
        P("fs", "sp", None),
        P("fs", "sp", None),
        P(),
        P(),
        P("tp", "fs"),
        P("tp", "fs"),
    )
    return jax.shard_map(
        functools.partial(local, mesh.shape["fs"], mesh.shape["sp"]),
        mesh=mesh,
        in_specs=placed,
        out_specs=(P("fs", ("sp", "tp"), None), P("fs", "sp", "tp")),
        check_vma=False,
    )
```

time: 39.1 us -> 30.9 us (0.79)
  Pallas kernels: 35.8 us -> 28.7 us
  local copies, waits for them, and re-layouts: 2.48 us -> 1.39 us
    pallas_call x1, Pallas kernels: 35.8 us -> 28.7 us  [local(): pl.pallas_call(functools.partial(kernel, (n_fs, span)), out_shape=(vmem((...]
    unnamed x4 -> x2, local copies, waits for them, and re-layouts: 2.48 us -> 1.39 us
where the time goes in v2:
time: 30.9 us; the launch traced here: 30.7 us
  Pallas kernels  28.7 us (93%)
  local copies, waits for them, and re-layouts  1.39 us (4%)
  between operations  0.64 us (2%)
    pallas_call x1, Pallas kernels, local(): pl.pallas_call(functools.partial(kernel, (n_fs, span)), out_shape=(vmem((...  28.7 us
    unnamed x2, local copies, waits for them, and re-layouts  1.39 us

profile of v2, /device:TPU:0, one launch (start us, length us, event | category | flops | bytes accessed | tf_op | source)
XLA Modules:
  0.0 30.7 jit_solution(6528399143134412759)
XLA Ops:
  0.6 28.7 %mixers.1 = (bf16[128,2048]{1,0:T(8,128)(2,1)S(1)}, f32[4,256]{1,0:T(4,128)S(1)}) custom-call(bf16[256,512]{1,0:T(8,128)(2,1)} %bitcast.19, bf16[256,512]{1,0:T(8,128)(2,1)} %bitcast.20, bf16[256,512]{1,0:T(8,128)(2,1)} %bitcast.21, f32[2,512]{1,0:T(2,128)} %floor_hbm.1, f32[4,256]{1,0:T(4,128)} %bitcast.25, f32[1,512]{1,0:T(1,128)} %bitcast.26, ...), custom_call_target="tpu_custom_call" | custom-call | tf_op jit(solution)/shard_map/mixers/pallas_call | solution.py:603
  29.4 0.8 %copy.21 = bf16[1,128,2048]{2,1,0:T(8,128)(2,1)} copy(bf16[1,128,2048]{2,1,0:T(8,128)(2,1)S(1)} %bitcast.17) | data formatting | bytes 1048576
  30.1 0.6 %copy.22 = f32[1,256,4]{1,2,0:T(4,128)} copy(f32[1,256,4]{1,2,0:T(4,128)S(1)} %bitcast.18) | data formatting | bytes 8192

commit v3 on v2

--- a/solution.py
+++ b/solution.py
@@ -76,21 +76,19 @@
     count = groups * cuts
     paired = span % 2 == 0
     if n_fs == 4 and paired:
-        direct = count - count // 3
-        lists = {1: list(range(direct)), 2: list(range(count - 1, count - 1 - direct, -1))}
+        direct = {1: count - count // 4, 2: count - count // 3}
+        lists = {1: list(range(direct[1])), 2: list(range(count - 1, count - 1 - direct[2], -1))}
         half = count // 2
-        cross = [(1, v) for v in range(half)], [(2, v) for v in range(count - 1, half - 1, -1)]
-        over = [(1, v) for v in range(count - direct)], [(2, v) for v in range(count - 1, direct - 1, -1)]
-        crosses = [[c[k] for c in cross] for k in range(half)]
-        pairs = [c[k] for k in range(count - direct) for c in over]
-        when = {}
-        for k in range(direct):
-            when[1, lists[1][k]] = when[2, lists[2][k]] = k + 1
-        for k in range(half):
-            when[3, cross[0][k][1]] = when[3, cross[1][k][1]] = direct + k + 1
-        for k in range(count - direct):
-            when[1, count - 1 - over[0][k][1]] = 5 + 2 * k
-            when[2, count - 1 - over[1][k][1]] = 6 + 2 * k
+        by_y = [(1, v, None) for v in range(half)] + [(1, half, 0)]
+        by_x = [(2, v, None) for v in range(count - 1, half, -1)] + [(2, half, 1)]
+        crosses = [by_y[k : k + 1] + (by_x[k - 1 : k] if k > 0 else []) for k in range(len(by_y))]
+        pairs = [(1, v) for v in range(count - direct[1])] + [(2, v) for v in range(count - 1, direct[2] - 1, -1)]
+        when = {(j, v): k + 1 for j in lists for k, v in enumerate(lists[j])}
+        for k, step in enumerate(crosses):
+            for _, v, _ in step:
+                when[3, v] = max(direct.values()) + k
+        for k, (j, v) in enumerate(pairs):
+            when[j, count - 1 - v] = half + 2 + k
     else:
         lists = {j: list(range(count)) for j in range(1, n_fs)}
         crosses, pairs = [], []
@@ -110,20 +108,31 @@
     return lists, crosses, pairs, batches
 
 
+def arrival_slots(n_fs, groups, cuts, crosses, pairs):
+    relayed = set(pairs) | {(j, v) for step in crosses for j, v, _ in step}
+    slots = {}
+    for j in range(1, n_fs):
+        for g in range(groups):
+            chunks = range(g * cuts, (g + 1) * cuts)
+            for v in chunks if any((j, v) in relayed for v in chunks) else chunks[:1]:
+                slots[j, v] = len(slots)
+    return slots
+
+
 def kernel(
     sizes,
     q_hbm, f_hbm, v_hbm, floor_hbm, extra_hbm, gain_hbm, aq_hbm, lat_hbm, rk_hbm,
     lgain_hbm, wup_hbm, cos_hbm, sin_hbm, turn_hbm, spread_hbm, w1_hbm, w2_hbm,
     out_ref, logw_ref,
-    q_ref, f_ref, v_ref, floor_ref, extra_ref, gain_ref, aq_ref, lat_ref, rk_ref,
-    lgain_ref, wup_ref, cos_ref, sin_ref, turn_ref, spread_ref,
+    qfv_ref, floor_ref, extra_ref, gain_ref, aq_ref, lat_ref, rk_ref,
+    lgain_ref, wup_ref, cs_ref, turn_ref, spread_ref,
     lbuf, ssend, srecv, wbuf, psend, precv, keep,
     kbuf, vbuf, intra, qd_ref, kd_ref, qc_ref, st_ref, act, whole_state, whole_decay,
     in_sem, own_sem, l_send, l_recv, f_send, f_recv, s_send, s_recv, w_send, w_recv,
     x_send, x_recv,
 ):
     n_fs, span = sizes
-    tokens, width = q_ref.shape
+    _, tokens, width = qfv_ref.shape
     heads = width // HG_DK
     att_heads = aq_ref.shape[1] // HEAD
     up = att_heads * (NOPE + VDIM)
@@ -156,19 +165,23 @@
         g, b = divmod(v, cuts)
         return g + parity * (groups - 1 - 2 * g), b + parity * (cuts - 1 - 2 * b)
 
-    def chunk(j, v):
+    def chunk(j, v, part=None):
         g, b = at_chunk(v)
-        return wbuf.at[j, pl.ds(pl.multiple_of(b * cut_rows, cut_rows), cut_rows),
-                       pl.ds(pl.multiple_of(g * LANES, LANES), LANES)]
-
-    relayed = set(pairs).union(*crosses)
+        first, size = b * cut_rows, cut_rows
+        if part is not None:
+            size = cut_rows // 2
+            first = first + part * size
+        return wbuf.at[j, pl.ds(pl.multiple_of(first, size), size), pl.ds(pl.multiple_of(g * LANES, LANES), LANES)]
+
+    slots = arrival_slots(n_fs, groups, cuts, crosses, pairs)
 
     def alone(j, v):
-        return any((j, v - v % cuts + b) in relayed for b in range(cuts))
+        return (j, v - v % cuts + 1) in slots
 
     def arrival(j, v, seen):
-        g, b = at_chunk(v)
-        return w_recv.at[j - 1, g * cuts + (b if alone(j, seen) else 0)]
+        if not alone(j, seen):
+            seen -= seen % cuts
+        return w_recv.at[slots[j, seen]]
 
     def remote(src, dst, send, recv, device):
         return pltpu.make_async_remote_copy(
@@ -180,7 +193,7 @@
         return pltpu.make_async_copy(src, dst, in_sem.at[k])
 
     own = [
-        pltpu.make_async_copy(src, wbuf.at[0, pl.ds(at, src.shape[0]), :], own_sem.at[k])
+        pltpu.make_async_copy(src, wbuf.at[0, pl.ds(at, src.shape[0]), :], own_sem.at[0])
         for k, (src, at) in enumerate(((w1_hbm, 0), (w2_hbm, w1_hbm.shape[0])))
     ]
     for c in own:
@@ -191,16 +204,16 @@
         fetch(0, lat_hbm, lat_ref), fetch(1, rk_hbm, rk_ref), fetch(2, lgain_hbm, lgain_ref),
         fetch(3, turn_hbm.at[:, my_tokens], turn_ref),
     ]
+    qfv = [fetch(6, src, qfv_ref.at[k]) for k, src in enumerate((q_hbm, f_hbm, v_hbm))]
+    turning = [fetch(7, src.at[my_tokens, :], cs_ref.at[k]) for k, src in enumerate((cos_hbm, sin_hbm))]
     gates = [
-        fetch(4, f_hbm, f_ref), fetch(5, q_hbm, q_ref), fetch(6, v_hbm, v_ref),
-        fetch(7, floor_hbm, floor_ref), fetch(8, extra_hbm, extra_ref),
+        fetch(4, floor_hbm, floor_ref), fetch(5, extra_hbm, extra_ref),
     ]
     late = [
-        fetch(9, gain_hbm, gain_ref), fetch(10, aq_hbm, aq_ref), fetch(11, wup_hbm.at[:, tp_up], wup_ref),
-        fetch(12, cos_hbm.at[my_tokens, :], cos_ref), fetch(13, sin_hbm.at[my_tokens, :], sin_ref),
-        fetch(14, spread_hbm, spread_ref),
+        fetch(8, gain_hbm, gain_ref), fetch(9, aq_hbm, aq_ref), fetch(10, wup_hbm.at[:, tp_up], wup_ref),
+        fetch(11, spread_hbm, spread_ref),
     ]
-    for c in early + gates + late:
+    for c in early + qfv + gates + turning + late:
         c.start()
 
     barrier = pltpu.get_barrier_semaphore()
@@ -241,7 +254,7 @@
         return remote(lbuf.at[at, tp], lbuf.at[at, tp], l_send.at[d, at], l_recv.at[at], right if d == 0 else left)
 
     def across(at):
-        return remote(lbuf.at[at, tp], lbuf.at[at, tp], f_send.at[at], f_recv.at[at], partner)
+        return remote(lbuf.at[at, tp], lbuf.at[at, tp], f_send.at[0], f_recv.at[at], partner)
 
     def latent_round(r):
         for d in range(2):
@@ -257,8 +270,7 @@
                 def _():
                     along(d, at).start()
 
-    for c in own:
-        c.wait()
+    pltpu.make_async_copy(wbuf.at[0], wbuf.at[0], own_sem.at[0]).wait()
     pl.semaphore_wait(barrier, len(direct) + 1 + has_left.astype(jnp.int32) + has_right.astype(jnp.int32))
     latent_round(0)
     for k in range(max((len(direct[j]) for j in direct), default=0)):
@@ -281,9 +293,9 @@
 
     def relay_cross(*ks):
         for k in ks:
-            for j, v in crosses[k] if k < len(crosses) else ():
+            for j, v, part in crosses[k] if k < len(crosses) else ():
                 await_chunk(j, v)
-                remote(chunk(j, v), chunk(3, v), w_send.at[0], arrival(3, v, v), fs_peer(3 - j)).start()
+                remote(chunk(j, v, part), chunk(3, v, part), w_send.at[0], arrival(3, v, v), fs_peer(3 - j)).start()
 
     def relay_pair(lo, hi):
         for j, v in pairs[lo:hi]:
@@ -291,11 +303,25 @@
             seen = groups * cuts - 1 - v
             remote(chunk(j, v), chunk(j, v), w_send.at[0], arrival(j, v, seen), pair).start()
 
+    held_from = max(len(crosses) - 2, 0)
+    held_pair = max(len(pairs) - 1, 0)
+
+    def relay_held():
+        relay_cross(*range(held_from, len(crosses)))
+        relay_pair(held_pair, len(pairs))
+
+    def await_held():
+        for j, v, _ in (one for step in crosses[held_from:] for one in step):
+            await_chunk(j, v)
+        for j, v in pairs[held_pair:]:
+            await_chunk(j, v)
+
     row = lax.broadcasted_iota(jnp.int32, (BLOCK, BLOCK), 0)
     col = lax.broadcasted_iota(jnp.int32, (BLOCK, BLOCK), 1)
     lower = row >= col
     upper = row <= col
     tri = (jnp.where(lower, 1.0, 0.0).astype(BF16), jnp.where(upper, 1.0, 0.0).astype(BF16))
+    fetch(6, qfv_ref, qfv_ref).wait()
     for c in gates:
         c.wait()
     spikes = lax.dot_general(
@@ -343,8 +369,8 @@
         wide_lanes = slice(h0 * HG_DK, (h0 + ahead) * HG_DK)
         for b in range(blocks):
             tok = slice(b * BLOCK, (b + 1) * BLOCK)
-            q = q_ref[tok, wide_lanes].astype(F32)
-            miss = 1.0 / (1.0 + jnp.exp(f_ref[tok, wide_lanes].astype(F32)))
+            q = qfv_ref[0, tok, wide_lanes].astype(F32)
+            miss = 1.0 / (1.0 + jnp.exp(qfv_ref[1, tok, wide_lanes].astype(F32)))
             spike = spikes[tok, wide_lanes]
             ending = []
             for d in range(2):
@@ -372,7 +398,7 @@
                 h = h0 + i
                 one = slice(i * HG_DK, (i + 1) * HG_DK)
                 both = jnp.concatenate([e[:, one] for e in ending], axis=1)
-                st_ref[b, h] = mm_tn(v_ref[tok, h * HG_DK : (h + 1) * HG_DK], both)
+                st_ref[b, h] = mm_tn(qfv_ref[2, tok, h * HG_DK : (h + 1) * HG_DK], both)
         for h in range(h0, h0 + ahead):
             for d in range(2):
                 side = slice(d * HG_DK, (d + 1) * HG_DK)
@@ -386,13 +412,14 @@
                 whole_state[d, h] = total
                 whole_decay[d, h] = jnp.broadcast_to(decay_all, (8, HG_DK))
 
-    if span > 1:
-        latent_round(1)
-    relay_pair(0, 2)
-
     @pl.when(jnp.logical_not(has_previous(first)))
     def _():
         pass_on(first)
+
+    relay_pair(0, 1)
+    if span > 1:
+        latent_round(1)
+    relay_pair(1, 2)
 
     for h in range(heads):
         lanes = slice(h * HG_DK, (h + 1) * HG_DK)
@@ -403,8 +430,9 @@
                 s = mm_nt(qd_ref[d, tok, lanes], kd_ref[d, tok, lanes])
                 s = jnp.where(lower if d == 0 else upper, s, 0.0)
                 scores = s if scores is None else scores + s
-            intra[tok, lanes] = mm(scores.astype(BF16), v_ref[tok, lanes])
-
+            intra[tok, lanes] = mm(scores.astype(BF16), qfv_ref[2, tok, lanes])
+
+    fetch(7, cs_ref, cs_ref).wait()
     for c in late:
         c.wait()
     wup = wup_ref[...]
@@ -449,7 +477,7 @@
     def act_slot(t):
         return t + tp * (1 - 2 * t)
 
-    cos, sin = cos_ref[...], sin_ref[...]
+    cos, sin = cs_ref[0], cs_ref[1]
     scale = HEAD ** (-0.5)
     lane = lax.broadcasted_iota(jnp.int32, (tokens, LANES), 1)
     logw = jnp.zeros((tokens, LANES), F32)
@@ -477,9 +505,14 @@
                 def _():
                     pass_on(1 - first)
 
-                relay_pair(3, len(pairs))
-                relay_cross(5)
-    relay_cross(*range(6, len(crosses)))
+                relay_pair(3, held_pair)
+    relay_cross(*range(5, held_from))
+    await_held()
+
+    @pl.when(tp == 0)
+    def _():
+        relay_held()
+
     logw_ref[...] = jnp.transpose(logw)[:att_heads]
 
     @pl.when(jnp.logical_not(has_next(1 - first)))
@@ -526,6 +559,11 @@
             if j > 0:
                 for v in range(g * cuts, (g + many) * cuts):
                     await_chunk(j, v)
+        if n == 1:
+            @pl.when(tp != 0)
+            def _():
+                relay_held()
+
         start = offset
         for j, g, many in batch:
             w = many * LANES
@@ -535,7 +573,7 @@
             offset += w
         part = slice(start, offset)
         spans.append((start, offset))
-        c = remote(psend.at[:, part], precv.at[:, part], x_send.at[n], x_recv.at[n], partner)
+        c = remote(psend.at[:, part], precv.at[:, part], x_send.at[0], x_recv.at[n], partner)
         c.start()
         x_copies.append(c)
         if n > 0:
@@ -543,18 +581,15 @@
     finish(len(batches) - 1)
 
     if direct:
-        remote(wbuf.at[1:], wbuf.at[1:], w_send.at[0], w_recv.at[0, 0], partner).wait_send()
-    for c in x_copies:
-        c.wait_send()
-
+        remote(wbuf.at[1:], wbuf.at[1:], w_send.at[0], w_recv.at[0], partner).wait_send()
+    remote(psend, precv, x_send.at[0], x_recv.at[0], partner).wait_send()
+
+    if span > 1:
+        all_across = lbuf.at[: span - 1, 0]
+        remote(all_across, all_across, f_send.at[0], f_recv.at[0], partner).wait_send()
     for r in range(span):
         for d in range(2):
             at, there, onward = source(d, r)
-            if r > 0:
-                @pl.when(there)
-                def _():
-                    across(at).wait_send()
-
             if r < span - 1:
                 @pl.when(onward)
                 def _():
@@ -594,7 +629,9 @@
     blocks = tokens // BLOCK
     rows = tokens // 2
     groups = columns // LANES
-    chunks = groups * (width // att_width + 1)
+    cuts = width // att_width + 1
+    _, crosses, pairs, _ = transfer_plan(n_fs, span, groups, cuts)
+    slots = len(arrival_slots(n_fs, groups, cuts, crosses, pairs))
     cos_pad, sin_pad, turns, spread = rope_constants(span * tokens, att_heads)
     vmem = pltpu.VMEM
     whole = pl.BlockSpec(memory_space=vmem)
@@ -609,11 +646,11 @@
         in_specs=[hbm] * 17,
         out_specs=(whole, whole),
         scratch_shapes=[
-            vmem((tokens, width), BF16), vmem((tokens, width), BF16), vmem((tokens, width), BF16),
+            vmem((3, tokens, width), BF16),
             vmem((2, width), F32), vmem((heads, tokens), F32), vmem((1, width), F32),
             vmem((tokens, att_heads * HEAD), BF16), vmem((tokens, latent_width), BF16), vmem((ROPE, tokens), BF16),
             vmem((1, latent_width), F32), vmem((latent_width, up), BF16),
-            vmem((tokens, LANES), F32), vmem((tokens, LANES), F32), vmem((ROPE, tokens), F32),
+            vmem((2, tokens, LANES), F32), vmem((ROPE, tokens), F32),
             vmem(spread.shape, BF16),
             vmem((span, 2, rows + ROPE // 2, latent_width), BF16),
             vmem((2, heads, HG_DK, HG_DK), BF16),
@@ -632,10 +669,10 @@
             vmem((2, rows, width + att_width), BF16),
             vmem((2, heads, HG_DK, HG_DK), F32),
             vmem((2, heads, 8, HG_DK), F32),
-            dma((15,)), dma((2,)), dma((2, span)), dma((span,)), dma((span,)), dma((span,)),
+            dma((12,)), dma((1,)), dma((2, span)), dma((span,)), dma((1,)), dma((span,)),
             dma((2,)), dma((2, heads)),
-            dma((1,)), dma((max(n_fs - 1, 1), chunks)),
-            dma((3,)), dma((3,)),
+            dma((1,)), dma((max(slots, 1),)),
+            dma((1,)), dma((3,)),
         ],
         compiler_params=pltpu.CompilerParams(
             collective_id=0, has_side_effects=True, vmem_limit_bytes=56 * 2**20

time: 30.9 us -> 29.9 us (0.968)
  Pallas kernels: 28.7 us -> 27.7 us
    pallas_call x1, Pallas kernels: 28.7 us -> 27.7 us  [local(): pl.pallas_call(functools.partial(kernel, (n_fs, span)), out_shape=(vmem((...]
where the time goes in v3:
time: 29.9 us; the launch traced here: 29.8 us
  Pallas kernels  27.7 us (93%)
  local copies, waits for them, and re-layouts  1.39 us (5%)
  between operations  0.64 us (2%)
    pallas_call x1, Pallas kernels, local(): pl.pallas_call(functools.partial(kernel, (n_fs, span)), out_shape=(vmem((...  27.7 us
    unnamed x2, local copies, waits for them, and re-layouts  1.39 us

profile of v3, /device:TPU:0, one launch (start us, length us, event | category | flops | bytes accessed | tf_op | source)
XLA Modules:
  0.0 29.8 jit_solution(9279279088264837903)
XLA Ops:
  0.6 27.7 %mixers.1 = (bf16[128,2048]{1,0:T(8,128)(2,1)S(1)}, f32[4,256]{1,0:T(4,128)S(1)}) custom-call(bf16[256,512]{1,0:T(8,128)(2,1)} %bitcast.19, bf16[256,512]{1,0:T(8,128)(2,1)} %bitcast.20, bf16[256,512]{1,0:T(8,128)(2,1)} %bitcast.21, f32[2,512]{1,0:T(2,128)} %floor_hbm.1, f32[4,256]{1,0:T(4,128)} %bitcast.25, f32[1,512]{1,0:T(1,128)} %bitcast.26, ...), custom_call_target="tpu_custom_call" | custom-call | tf_op jit(solution)/shard_map/mixers/pallas_call | solution.py:640
  28.4 0.8 %copy.21 = bf16[1,128,2048]{2,1,0:T(8,128)(2,1)} copy(bf16[1,128,2048]{2,1,0:T(8,128)(2,1)S(1)} %bitcast.17) | data formatting | bytes 1048576
  29.2 0.6 %copy.22 = f32[1,256,4]{1,2,0:T(4,128)} copy(f32[1,256,4]{1,2,0:T(4,128)S(1)} %bitcast.18) | data formatting | bytes 8192

commit v4 on v3

--- a/solution.py
+++ b/solution.py
@@ -505,8 +505,8 @@
                 def _():
                     pass_on(1 - first)
 
-                relay_pair(3, held_pair)
-    relay_cross(*range(5, held_from))
+                relay_pair(3, max(held_pair, 3))
+    relay_cross(*range(5, max(held_from, 5)))
     await_held()
 
     @pl.when(tp == 0)
@@ -599,6 +599,17 @@
         @pl.when(has_next(d))
         def _():
             remote(ssend.at[d], srecv.at[d], s_send.at[d], s_recv.at[d, 0], partner).wait_send()
+
+
+def flush(mixed_ref, logw_ref, mixed_hbm, logw_hbm, sems):
+    copies = (
+        pltpu.make_async_copy(mixed_ref, mixed_hbm, sems.at[0]),
+        pltpu.make_async_copy(logw_ref, logw_hbm, sems.at[1]),
+    )
+    for c in copies:
+        c.start()
+    for c in copies:
+        c.wait()
 
 
 def local(
@@ -697,6 +708,19 @@
         recurrent_output_weight,
         attention_output_weight,
     )
+    mixed = pltpu.with_memory_space_constraint(mixed, vmem)
+    log_weight = pltpu.with_memory_space_constraint(log_weight, vmem)
+    mixed, log_weight = pl.pallas_call(
+        flush,
+        out_shape=(
+            jax.ShapeDtypeStruct((rows, columns * n_fs), BF16),
+            jax.ShapeDtypeStruct((att_heads, tokens), F32),
+        ),
+        in_specs=[whole, whole],
+        out_specs=(hbm, hbm),
+        scratch_shapes=[dma((2,))],
+        name="flush",
+    )(mixed, log_weight)
     return mixed[None], log_weight.T[None]
 
 

time: 29.9 us -> 29.3 us (0.980)
  local copies, waits for them, and re-layouts: 1.39 us -> 0 us
  Pallas kernels: 27.7 us -> 28.5 us
    unnamed x2 -> x0, local copies, waits for them, and re-layouts: 1.39 us -> none
    pallas_call x0 -> x1, Pallas kernels: none -> 0.81 us  [local(): pl.pallas_call(flush, out_shape=(jax.ShapeDtypeStruct((rows, columns * n_...]
where the time goes in v4:
time: 29.3 us; the launch traced here: 29.2 us
  Pallas kernels  28.5 us (97%)
  between operations  0.64 us (2%)
    pallas_call x1, Pallas kernels, local(): pl.pallas_call(functools.partial(kernel, (n_fs, span)), out_shape=(vmem((...  27.7 us
    pallas_call x1, Pallas kernels, local(): pl.pallas_call(flush, out_shape=(jax.ShapeDtypeStruct((rows, columns * n_...  0.81 us

profile of v4, /device:TPU:0, one launch (start us, length us, event | category | flops | bytes accessed | tf_op | source)
XLA Modules:
  0.0 29.2 jit_solution(18198685450471592521)
XLA Ops:
  0.6 27.7 %mixers.1 = (bf16[128,2048]{1,0:T(8,128)(2,1)S(1)}, f32[4,256]{1,0:T(4,128)S(1)}) custom-call(bf16[256,512]{1,0:T(8,128)(2,1)} %bitcast.17, bf16[256,512]{1,0:T(8,128)(2,1)} %bitcast.18, bf16[256,512]{1,0:T(8,128)(2,1)} %bitcast.19, f32[2,512]{1,0:T(2,128)} %floor_hbm.1, f32[4,256]{1,0:T(4,128)} %bitcast.23, f32[1,512]{1,0:T(1,128)} %bitcast.24, ...), custom_call_target="tpu_custom_call" | custom-call | tf_op jit(solution)/shard_map/mixers/pallas_call | solution.py:651
  28.4 0.8 %flush.1 = (bf16[128,2048]{1,0:T(8,128)(2,1)}, f32[4,256]{1,0:T(4,128)}) custom-call(bf16[128,2048]{1,0:T(8,128)(2,1)S(1)} %get-tuple-element.6.mixed_ref, f32[4,256]{1,0:T(4,128)S(1)} %get-tuple-element.7.logw_ref), custom_call_target="tpu_custom_call" | custom-call | tf_op jit(solution)/shard_map/flush/pallas_call | solution.py:713

commit v5 on v4

--- a/solution.py
+++ b/solution.py
@@ -76,23 +76,26 @@
     count = groups * cuts
     paired = span % 2 == 0
     if n_fs == 4 and paired:
-        direct = {1: count - count // 4, 2: count - count // 3}
-        lists = {1: list(range(direct[1])), 2: list(range(count - 1, count - 1 - direct[2], -1))}
-        half = count // 2
-        by_y = [(1, v, None) for v in range(half)] + [(1, half, 0)]
-        by_x = [(2, v, None) for v in range(count - 1, half, -1)] + [(2, half, 1)]
+        third, half = count // 3, count // 2
+        keep = count - third
+        lists = {1: [(0, (0, 2)), (0, (2, 4))] + [(v, None) for v in range(1, keep)] + [(keep, (0, 2))],
+                 2: [(v, None) for v in range(count - 1, third - 1, -1)]}
+        by_y = [(1, v, None) for v in range(half)] + [(1, half, (0, 1))]
+        by_x = [(2, v, None) for v in range(count - 1, half, -1)] + [(2, half, (1, 4))]
         crosses = [by_y[k : k + 1] + (by_x[k - 1 : k] if k > 0 else []) for k in range(len(by_y))]
-        pairs = [(1, v) for v in range(count - direct[1])] + [(2, v) for v in range(count - 1, direct[2] - 1, -1)]
-        when = {(j, v): k + 1 for j in lists for k, v in enumerate(lists[j])}
+        pairs = [(1, 0, (0, 2)), (1, 0, (2, 4)), (2, count - 1, None)]
+        pairs += [(1, v, None) for v in range(1, third - 1)] + [(1, third - 1, (2, 4))]
+        pairs += [(2, v, None) for v in range(count - 2, keep - 1, -1)]
+        when = {(j, v): k + 1 for j in lists for k, (v, _) in enumerate(lists[j])}
         for k, step in enumerate(crosses):
             for _, v, _ in step:
-                when[3, v] = max(direct.values()) + k
-        for k, (j, v) in enumerate(pairs):
+                when[3, v] = keep + k
+        for k, (j, v, _) in enumerate(pairs):
             when[j, count - 1 - v] = half + 2 + k
     else:
-        lists = {j: list(range(count)) for j in range(1, n_fs)}
+        lists = {j: [(v, None) for v in range(count)] for j in range(1, n_fs)}
         crosses, pairs = [], []
-        when = {(j, v): v * n_fs + j for j in lists for v in lists[j]}
+        when = {(j, v): v * n_fs + j for j in lists for v, _ in lists[j]}
     last = {(j, g): max(when[j, g * cuts + b] for b in range(cuts)) for j in range(1, n_fs) for g in range(groups)}
     order = [(0, g) for g in range(groups)] + sorted(last, key=lambda one: (last[one], one))
     bounds = [0, len(order) // 2, 3 * len(order) // 4, len(order)]
@@ -109,13 +112,13 @@
 
 
 def arrival_slots(n_fs, groups, cuts, crosses, pairs):
-    relayed = set(pairs) | {(j, v) for step in crosses for j, v, _ in step}
+    relayed = {(j, v) for step in crosses + [pairs] for j, v, _ in step}
     slots = {}
     for j in range(1, n_fs):
         for g in range(groups):
             chunks = range(g * cuts, (g + 1) * cuts)
             for v in chunks if any((j, v) in relayed for v in chunks) else chunks[:1]:
-                slots[j, v] = len(slots)
+                slots[j, v] = len(slots) + (len(slots) > 0)
     return slots
 
 
@@ -167,21 +170,20 @@
 
     def chunk(j, v, part=None):
         g, b = at_chunk(v)
-        first, size = b * cut_rows, cut_rows
-        if part is not None:
-            size = cut_rows // 2
-            first = first + part * size
-        return wbuf.at[j, pl.ds(pl.multiple_of(first, size), size), pl.ds(pl.multiple_of(g * LANES, LANES), LANES)]
+        lo, hi = part or (0, 4)
+        quarter = cut_rows // 4
+        first = pl.multiple_of(b * cut_rows + lo * quarter, quarter)
+        return wbuf.at[j, pl.ds(first, (hi - lo) * quarter), pl.ds(pl.multiple_of(g * LANES, LANES), LANES)]
 
     slots = arrival_slots(n_fs, groups, cuts, crosses, pairs)
 
     def alone(j, v):
         return (j, v - v % cuts + 1) in slots
 
-    def arrival(j, v, seen):
+    def arrival(j, v, seen, part=None):
         if not alone(j, seen):
             seen -= seen % cuts
-        return w_recv.at[slots[j, seen]]
+        return w_recv.at[slots[j, seen] + ((j, seen) == (1, 0) and part == (2, 4))]
 
     def remote(src, dst, send, recv, device):
         return pltpu.make_async_remote_copy(
@@ -276,20 +278,26 @@
     for k in range(max((len(direct[j]) for j in direct), default=0)):
         for j in direct:
             if k < len(direct[j]):
-                v = direct[j][k]
-                remote(chunk(0, v), chunk(j, v), w_send.at[0], arrival(j, v, v), fs_peer(j)).start()
+                v, part = direct[j][k]
+                remote(chunk(0, v, part), chunk(j, v, part), w_send.at[0], arrival(j, v, v, part), fs_peer(j)).start()
     arrived = set()
 
-    def await_chunk(j, v):
+    def await_chunk(j, v, part=None):
         if not alone(j, v):
             v -= v % cuts
-        if (j, v) in arrived:
-            return
-        arrived.add((j, v))
-        ref = chunk(j, v)
-        if not alone(j, v):
-            ref = wbuf.at[j, :, pl.ds(pl.multiple_of(at_chunk(v)[0] * LANES, LANES), LANES)]
-        remote(ref, ref, w_send.at[0], arrival(j, v, v), partner).wait_recv()
+        halves = (part,)
+        if crosses and (j, v) == (1, 0) and part is None:
+            halves = ((0, 2), (2, 4))
+        elif (j, v) != (1, 0):
+            halves = (None,)
+        for one in halves:
+            if (j, v, one) in arrived:
+                continue
+            arrived.add((j, v, one))
+            ref = chunk(j, v, one)
+            if not alone(j, v):
+                ref = wbuf.at[j, :, pl.ds(pl.multiple_of(at_chunk(v)[0] * LANES, LANES), LANES)]
+            remote(ref, ref, w_send.at[0], arrival(j, v, v, one), partner).wait_recv()
 
     def relay_cross(*ks):
         for k in ks:
@@ -298,10 +306,10 @@
                 remote(chunk(j, v, part), chunk(3, v, part), w_send.at[0], arrival(3, v, v), fs_peer(3 - j)).start()
 
     def relay_pair(lo, hi):
-        for j, v in pairs[lo:hi]:
-            await_chunk(j, v)
+        for j, v, part in pairs[lo:hi]:
+            await_chunk(j, v, part)
             seen = groups * cuts - 1 - v
-            remote(chunk(j, v), chunk(j, v), w_send.at[0], arrival(j, v, seen), pair).start()
+            remote(chunk(j, v, part), chunk(j, v, part), w_send.at[0], arrival(j, v, seen), pair).start()
 
     held_from = max(len(crosses) - 2, 0)
     held_pair = max(len(pairs) - 1, 0)
@@ -311,9 +319,7 @@
         relay_pair(held_pair, len(pairs))
 
     def await_held():
-        for j, v, _ in (one for step in crosses[held_from:] for one in step):
-            await_chunk(j, v)
-        for j, v in pairs[held_pair:]:
+        for j, v, _ in sum(crosses[held_from:], pairs[held_pair:]):
             await_chunk(j, v)
 
     row = lax.broadcasted_iota(jnp.int32, (BLOCK, BLOCK), 0)
@@ -416,10 +422,10 @@
     def _():
         pass_on(first)
 
-    relay_pair(0, 1)
+    relay_pair(0, 3)
     if span > 1:
         latent_round(1)
-    relay_pair(1, 2)
+    relay_pair(3, 4)
 
     for h in range(heads):
         lanes = slice(h * HG_DK, (h + 1) * HG_DK)
@@ -458,7 +464,7 @@
     relay_cross(0, 1)
     if span > 2:
         latent_round(2)
-    relay_pair(2, 3)
+    relay_pair(4, 5)
     relay_cross(2)
 
     @pl.when(has_previous(first))
@@ -505,7 +511,7 @@
                 def _():
                     pass_on(1 - first)
 
-                relay_pair(3, max(held_pair, 3))
+                relay_pair(5, max(held_pair, 5))
     relay_cross(*range(5, max(held_from, 5)))
     await_held()
 
@@ -642,7 +648,7 @@
     groups = columns // LANES
     cuts = width // att_width + 1
     _, crosses, pairs, _ = transfer_plan(n_fs, span, groups, cuts)
-    slots = len(arrival_slots(n_fs, groups, cuts, crosses, pairs))
+    slots = len(arrival_slots(n_fs, groups, cuts, crosses, pairs)) + 1
     cos_pad, sin_pad, turns, spread = rope_constants(span * tokens, att_heads)
     vmem = pltpu.VMEM
     whole = pl.BlockSpec(memory_space=vmem)

time: 29.3 us -> 28.7 us (0.980)
  Pallas kernels: 28.5 us -> 27.9 us
    pallas_call x1, Pallas kernels: 27.7 us -> 27.1 us  [local(): pl.pallas_call(functools.partial(kernel, (n_fs, span)), out_shape=(vmem((...]
where the time goes in v5:
time: 28.7 us; the launch traced here: 28.6 us
  Pallas kernels  27.9 us (97%)
  between operations  0.64 us (2%)
    pallas_call x1, Pallas kernels, local(): pl.pallas_call(functools.partial(kernel, (n_fs, span)), out_shape=(vmem((...  27.1 us
    pallas_call x1, Pallas kernels, local(): pl.pallas_call(flush, out_shape=(jax.ShapeDtypeStruct((rows, columns * n_...  0.81 us

profile of v5, /device:TPU:0, one launch (start us, length us, event | category | flops | bytes accessed | tf_op | source)
XLA Modules:
  0.0 28.6 jit_solution(5234293894660368769)
XLA Ops:
  0.6 27.1 %mixers.1 = (bf16[128,2048]{1,0:T(8,128)(2,1)S(1)}, f32[4,256]{1,0:T(4,128)S(1)}) custom-call(bf16[256,512]{1,0:T(8,128)(2,1)} %bitcast.17, bf16[256,512]{1,0:T(8,128)(2,1)} %bitcast.18, bf16[256,512]{1,0:T(8,128)(2,1)} %bitcast.19, f32[2,512]{1,0:T(2,128)} %floor_hbm.1, f32[4,256]{1,0:T(4,128)} %bitcast.23, f32[1,512]{1,0:T(1,128)} %bitcast.24, ...), custom_call_target="tpu_custom_call" | custom-call | tf_op jit(solution)/shard_map/mixers/pallas_call | solution.py:657
  27.8 0.8 %flush.1 = (bf16[128,2048]{1,0:T(8,128)(2,1)}, f32[4,256]{1,0:T(4,128)}) custom-call(bf16[128,2048]{1,0:T(8,128)(2,1)S(1)} %get-tuple-element.6.mixed_ref, f32[4,256]{1,0:T(4,128)S(1)} %get-tuple-element.7.logw_ref), custom_call_target="tpu_custom_call" | custom-call | tf_op jit(solution)/shard_map/flush/pallas_call | solution.py:719

commit v6 on v5

--- a/solution.py
+++ b/solution.py
@@ -1,4 +1,5 @@
 import functools
+import math
 
 import jax
 import jax.numpy as jnp
@@ -91,14 +92,14 @@
             for _, v, _ in step:
                 when[3, v] = keep + k
         for k, (j, v, _) in enumerate(pairs):
-            when[j, count - 1 - v] = half + 2 + k
+            when[j, count - 1 - v] = half - 1 + k
     else:
         lists = {j: [(v, None) for v in range(count)] for j in range(1, n_fs)}
         crosses, pairs = [], []
         when = {(j, v): v * n_fs + j for j in lists for v, _ in lists[j]}
     last = {(j, g): max(when[j, g * cuts + b] for b in range(cuts)) for j in range(1, n_fs) for g in range(groups)}
     order = [(0, g) for g in range(groups)] + sorted(last, key=lambda one: (last[one], one))
-    bounds = [0, len(order) // 2, 3 * len(order) // 4, len(order)]
+    bounds = [len(order) * part // 8 for part in (0, 4, 6, 7, 8)]
     batches = []
     for lo, hi in zip(bounds, bounds[1:]):
         batch = []
@@ -132,7 +133,7 @@
     lbuf, ssend, srecv, wbuf, psend, precv, keep,
     kbuf, vbuf, intra, qd_ref, kd_ref, qc_ref, st_ref, act, whole_state, whole_decay,
     in_sem, own_sem, l_send, l_recv, f_send, f_recv, s_send, s_recv, w_send, w_recv,
-    x_send, x_recv,
+    x_send, x_recv, ruler,
 ):
     n_fs, span = sizes
     _, tokens, width = qfv_ref.shape
@@ -191,8 +192,26 @@
             device_id=device, device_id_type=mesh_id,
         )
 
+    def fetched(k, *refs):
+        size = sum(math.prod(ref.shape) * ref.dtype.itemsize for ref in refs)
+        ref = ruler.at[pl.ds(0, size // (4 * LANES)), :]
+        pltpu.make_async_copy(ref, ref, in_sem.at[k]).wait()
+
     def fetch(k, src, dst):
         return pltpu.make_async_copy(src, dst, in_sem.at[k])
+
+    barrier = pltpu.get_barrier_semaphore()
+    for j in direct:
+        pl.semaphore_signal(barrier, inc=1, device_id=fs_peer(j), device_id_type=mesh_id)
+    pl.semaphore_signal(barrier, inc=1, device_id=partner, device_id_type=mesh_id)
+
+    @pl.when(has_left)
+    def _():
+        pl.semaphore_signal(barrier, inc=1, device_id=left, device_id_type=mesh_id)
+
+    @pl.when(has_right)
+    def _():
+        pl.semaphore_signal(barrier, inc=1, device_id=right, device_id_type=mesh_id)
 
     own = [
         pltpu.make_async_copy(src, wbuf.at[0, pl.ds(at, src.shape[0]), :], own_sem.at[0])
@@ -203,36 +222,20 @@
     my_tokens = pl.ds(pl.multiple_of(place * tokens, tokens), tokens)
     tp_up = pl.ds(pl.multiple_of(tp * up, LANES), up)
     early = [
-        fetch(0, lat_hbm, lat_ref), fetch(1, rk_hbm, rk_ref), fetch(2, lgain_hbm, lgain_ref),
-        fetch(3, turn_hbm.at[:, my_tokens], turn_ref),
+        fetch(0, lat_hbm, lat_ref), fetch(0, rk_hbm, rk_ref), fetch(0, lgain_hbm, lgain_ref),
+        fetch(0, turn_hbm.at[:, my_tokens], turn_ref),
     ]
-    qfv = [fetch(6, src, qfv_ref.at[k]) for k, src in enumerate((q_hbm, f_hbm, v_hbm))]
-    turning = [fetch(7, src.at[my_tokens, :], cs_ref.at[k]) for k, src in enumerate((cos_hbm, sin_hbm))]
-    gates = [
-        fetch(4, floor_hbm, floor_ref), fetch(5, extra_hbm, extra_ref),
+    gates = [fetch(1, src, qfv_ref.at[k]) for k, src in enumerate((q_hbm, f_hbm, v_hbm))]
+    late = [fetch(2, src.at[my_tokens, :], cs_ref.at[k]) for k, src in enumerate((cos_hbm, sin_hbm))]
+    gates += [fetch(1, floor_hbm, floor_ref), fetch(1, extra_hbm, extra_ref)]
+    late += [
+        fetch(2, gain_hbm, gain_ref), fetch(2, aq_hbm, aq_ref), fetch(2, wup_hbm.at[:, tp_up], wup_ref),
+        fetch(2, spread_hbm, spread_ref),
     ]
-    late = [
-        fetch(8, gain_hbm, gain_ref), fetch(9, aq_hbm, aq_ref), fetch(10, wup_hbm.at[:, tp_up], wup_ref),
-        fetch(11, spread_hbm, spread_ref),
-    ]
-    for c in early + qfv + gates + turning + late:
+    for c in early + gates + late:
         c.start()
 
-    barrier = pltpu.get_barrier_semaphore()
-    for j in direct:
-        pl.semaphore_signal(barrier, inc=1, device_id=fs_peer(j), device_id_type=mesh_id)
-    pl.semaphore_signal(barrier, inc=1, device_id=partner, device_id_type=mesh_id)
-
-    @pl.when(has_left)
-    def _():
-        pl.semaphore_signal(barrier, inc=1, device_id=left, device_id_type=mesh_id)
-
-    @pl.when(has_right)
-    def _():
-        pl.semaphore_signal(barrier, inc=1, device_id=right, device_id_type=mesh_id)
-
-    for c in early:
-        c.wait()
+    fetched(0, lat_ref, rk_ref, lgain_ref, turn_ref)
     lat = lat_ref[...].astype(F32)
     normed = lat * lax.rsqrt(jnp.mean(lat * lat, axis=-1, keepdims=True) + norm_eps) * lgain_ref[...]
     normed = normed.astype(BF16)
@@ -253,7 +256,7 @@
         return jnp.clip(at, 0, span - 1), there, onward
 
     def along(d, at):
-        return remote(lbuf.at[at, tp], lbuf.at[at, tp], l_send.at[d, at], l_recv.at[at], right if d == 0 else left)
+        return remote(lbuf.at[at, tp], lbuf.at[at, tp], l_send.at[d], l_recv.at[at], right if d == 0 else left)
 
     def across(at):
         return remote(lbuf.at[at, tp], lbuf.at[at, tp], f_send.at[0], f_recv.at[at], partner)
@@ -327,9 +330,7 @@
     lower = row >= col
     upper = row <= col
     tri = (jnp.where(lower, 1.0, 0.0).astype(BF16), jnp.where(upper, 1.0, 0.0).astype(BF16))
-    fetch(6, qfv_ref, qfv_ref).wait()
-    for c in gates:
-        c.wait()
+    fetched(1, qfv_ref, floor_ref, extra_ref)
     spikes = lax.dot_general(
         extra_ref[...],
         jnp.where(
@@ -438,9 +439,7 @@
                 scores = s if scores is None else scores + s
             intra[tok, lanes] = mm(scores.astype(BF16), qfv_ref[2, tok, lanes])
 
-    fetch(7, cs_ref, cs_ref).wait()
-    for c in late:
-        c.wait()
+    fetched(2, cs_ref, gain_ref, aq_ref, wup_ref, spread_ref)
     wup = wup_ref[...]
     half_lane = lax.broadcasted_iota(jnp.int32, (rows, LANES), 1)
     put_a = spread_ref[0, NOPE : NOPE + half_rope, :LANES]
@@ -593,13 +592,16 @@
     if span > 1:
         all_across = lbuf.at[: span - 1, 0]
         remote(all_across, all_across, f_send.at[0], f_recv.at[0], partner).wait_send()
-    for r in range(span):
-        for d in range(2):
-            at, there, onward = source(d, r)
-            if r < span - 1:
-                @pl.when(onward)
-                def _():
-                    along(d, at).wait_send()
+    for k in range(span - 1):
+        passed = lbuf.at[: k + 1, 0]
+
+        @pl.when(place == k)
+        def _():
+            remote(passed, passed, l_send.at[0], l_recv.at[0], partner).wait_send()
+
+        @pl.when(place == span - 1 - k)
+        def _():
+            remote(passed, passed, l_send.at[1], l_recv.at[0], partner).wait_send()
 
     for d in range(2):
         @pl.when(has_next(d))
@@ -608,14 +610,14 @@
 
 
 def flush(mixed_ref, logw_ref, mixed_hbm, logw_hbm, sems):
-    copies = (
-        pltpu.make_async_copy(mixed_ref, mixed_hbm, sems.at[0]),
-        pltpu.make_async_copy(logw_ref, logw_hbm, sems.at[1]),
-    )
-    for c in copies:
-        c.start()
-    for c in copies:
-        c.wait()
+    logw_copy = pltpu.make_async_copy(logw_ref, logw_hbm, sems.at[1])
+    logw_copy.start()
+    size = mixed_ref.shape[0] // 4
+    for k in range(4):
+        part = pl.ds(k * size, size)
+        pltpu.make_async_copy(mixed_ref.at[part], mixed_hbm.at[part], sems.at[0]).start()
+    logw_copy.wait()
+    pltpu.make_async_copy(mixed_ref, mixed_hbm, sems.at[0]).wait()
 
 
 def local(
@@ -686,10 +688,11 @@
             vmem((2, rows, width + att_width), BF16),
             vmem((2, heads, HG_DK, HG_DK), F32),
             vmem((2, heads, 8, HG_DK), F32),
-            dma((12,)), dma((1,)), dma((2, span)), dma((span,)), dma((1,)), dma((span,)),
+            dma((3,)), dma((1,)), dma((2,)), dma((span,)), dma((1,)), dma((span,)),
             dma((2,)), dma((2, heads)),
             dma((1,)), dma((max(slots, 1),)),
-            dma((1,)), dma((3,)),
+            dma((1,)), dma((4,)),
+            vmem((4096, LANES), F32),
         ],
         compiler_params=pltpu.CompilerParams(
             collective_id=0, has_side_effects=True, vmem_limit_bytes=56 * 2**20

time: 28.7 us -> 28.6 us (level)
  no operation moved by 1% of the time
where the time goes in v6:
time: 28.6 us; the launch traced here: 28.4 us
  Pallas kernels  27.8 us (97%)
  between operations  0.64 us (2%)
    pallas_call x1, Pallas kernels, local(): pl.pallas_call(functools.partial(kernel, (n_fs, span)), out_shape=(vmem((...  27 us
    pallas_call x1, Pallas kernels, local(): pl.pallas_call(flush, out_shape=(jax.ShapeDtypeStruct((rows, columns * n_...  0.81 us

profile of v6, /device:TPU:0, one launch (start us, length us, event | category | flops | bytes accessed | tf_op | source)
XLA Modules:
  0.0 28.4 jit_solution(8381151889197454855)
XLA Ops:
  0.6 27.0 %mixers.1 = (bf16[128,2048]{1,0:T(8,128)(2,1)S(1)}, f32[4,256]{1,0:T(4,128)S(1)}) custom-call(bf16[256,512]{1,0:T(8,128)(2,1)} %bitcast.17, bf16[256,512]{1,0:T(8,128)(2,1)} %bitcast.18, bf16[256,512]{1,0:T(8,128)(2,1)} %bitcast.19, f32[2,512]{1,0:T(2,128)} %floor_hbm.1, f32[4,256]{1,0:T(4,128)} %bitcast.23, f32[1,512]{1,0:T(1,128)} %bitcast.24, ...), custom_call_target="tpu_custom_call" | custom-call | tf_op jit(solution)/shard_map/mixers/pallas_call | solution.py:659
  27.6 0.8 %flush.1 = (bf16[128,2048]{1,0:T(8,128)(2,1)}, f32[4,256]{1,0:T(4,128)}) custom-call(bf16[128,2048]{1,0:T(8,128)(2,1)S(1)} %get-tuple-element.6.mixed_ref, f32[4,256]{1,0:T(4,128)S(1)} %get-tuple-element.7.logw_ref), custom_call_target="tpu_custom_call" | custom-call | tf_op jit(solution)/shard_map/flush/pallas_call | solution.py:722

commit v7 on v6

--- a/solution.py
+++ b/solution.py
@@ -79,14 +79,14 @@
     if n_fs == 4 and paired:
         third, half = count // 3, count // 2
         keep = count - third
-        lists = {1: [(0, (0, 2)), (0, (2, 4))] + [(v, None) for v in range(1, keep)] + [(keep, (0, 2))],
-                 2: [(v, None) for v in range(count - 1, third - 1, -1)]}
-        by_y = [(1, v, None) for v in range(half)] + [(1, half, (0, 1))]
-        by_x = [(2, v, None) for v in range(count - 1, half, -1)] + [(2, half, (1, 4))]
+        lists = {1: [(0, (0, 4)), (0, (4, 8))] + [(v, None) for v in range(1, keep)] + [(keep, (0, 4))],
+                 2: [(v, None) for v in range(count - 1, third, -1)] + [(third, (0, 6))]}
+        by_y = [(1, v, None) for v in range(half)] + [(1, half, (0, 3))]
+        by_x = [(2, v, None) for v in range(count - 1, half, -1)] + [(2, half, (3, 8))]
         crosses = [by_y[k : k + 1] + (by_x[k - 1 : k] if k > 0 else []) for k in range(len(by_y))]
-        pairs = [(1, 0, (0, 2)), (1, 0, (2, 4)), (2, count - 1, None)]
-        pairs += [(1, v, None) for v in range(1, third - 1)] + [(1, third - 1, (2, 4))]
-        pairs += [(2, v, None) for v in range(count - 2, keep - 1, -1)]
+        pairs = [(1, 0, (0, 4)), (1, 0, (4, 8)), (2, count - 1, None)]
+        pairs += [(1, v, None) for v in range(1, third - 1)] + [(1, third - 1, (4, 8))]
+        pairs += [(2, v, None) for v in range(count - 2, keep - 1, -1)] + [(2, keep - 1, (6, 8))]
         when = {(j, v): k + 1 for j in lists for k, (v, _) in enumerate(lists[j])}
         for k, step in enumerate(crosses):
             for _, v, _ in step:
@@ -171,10 +171,10 @@
 
     def chunk(j, v, part=None):
         g, b = at_chunk(v)
-        lo, hi = part or (0, 4)
-        quarter = cut_rows // 4
-        first = pl.multiple_of(b * cut_rows + lo * quarter, quarter)
-        return wbuf.at[j, pl.ds(first, (hi - lo) * quarter), pl.ds(pl.multiple_of(g * LANES, LANES), LANES)]
+        lo, hi = part or (0, 8)
+        eighth = cut_rows // 8
+        first = pl.multiple_of(b * cut_rows + lo * eighth, eighth)
+        return wbuf.at[j, pl.ds(first, (hi - lo) * eighth), pl.ds(pl.multiple_of(g * LANES, LANES), LANES)]
 
     slots = arrival_slots(n_fs, groups, cuts, crosses, pairs)
 
@@ -184,7 +184,7 @@
     def arrival(j, v, seen, part=None):
         if not alone(j, seen):
             seen -= seen % cuts
-        return w_recv.at[slots[j, seen] + ((j, seen) == (1, 0) and part == (2, 4))]
+        return w_recv.at[slots[j, seen] + ((j, seen) == (1, 0) and part == (4, 8))]
 
     def remote(src, dst, send, recv, device):
         return pltpu.make_async_remote_copy(
@@ -290,7 +290,7 @@
             v -= v % cuts
         halves = (part,)
         if crosses and (j, v) == (1, 0) and part is None:
-            halves = ((0, 2), (2, 4))
+            halves = ((0, 4), (4, 8))
         elif (j, v) != (1, 0):
             halves = (None,)
         for one in halves:
@@ -315,7 +315,7 @@
             remote(chunk(j, v, part), chunk(j, v, part), w_send.at[0], arrival(j, v, seen), pair).start()
 
     held_from = max(len(crosses) - 2, 0)
-    held_pair = max(len(pairs) - 1, 0)
+    held_pair = max(len(pairs) - 2, 0)
 
     def relay_held():
         relay_cross(*range(held_from, len(crosses)))

time: 28.6 us -> 28.5 us (level)
  no operation moved by 1% of the time
where the time goes in v7:
time: 28.5 us; the launch traced here: 28.4 us
  Pallas kernels  27.8 us (98%)
  between operations  0.64 us (2%)
    pallas_call x1, Pallas kernels, local(): pl.pallas_call(functools.partial(kernel, (n_fs, span)), out_shape=(vmem((...  26.9 us
    pallas_call x1, Pallas kernels, local(): pl.pallas_call(flush, out_shape=(jax.ShapeDtypeStruct((rows, columns * n_...  0.81 us

profile of v7, /device:TPU:0, one launch (start us, length us, event | category | flops | bytes accessed | tf_op | source)
XLA Modules:
  0.0 28.4 jit_solution(7320885036350485884)
XLA Ops:
  0.6 26.9 %mixers.1 = (bf16[128,2048]{1,0:T(8,128)(2,1)S(1)}, f32[4,256]{1,0:T(4,128)S(1)}) custom-call(bf16[256,512]{1,0:T(8,128)(2,1)} %bitcast.17, bf16[256,512]{1,0:T(8,128)(2,1)} %bitcast.18, bf16[256,512]{1,0:T(8,128)(2,1)} %bitcast.19, f32[2,512]{1,0:T(2,128)} %floor_hbm.1, f32[4,256]{1,0:T(4,128)} %bitcast.23, f32[1,512]{1,0:T(1,128)} %bitcast.24, ...), custom_call_target="tpu_custom_call" | custom-call | tf_op jit(solution)/shard_map/mixers/pallas_call | solution.py:659
  27.6 0.8 %flush.1 = (bf16[128,2048]{1,0:T(8,128)(2,1)}, f32[4,256]{1,0:T(4,128)}) custom-call(bf16[128,2048]{1,0:T(8,128)(2,1)S(1)} %get-tuple-element.6.mixed_ref, f32[4,256]{1,0:T(4,128)S(1)} %get-tuple-element.7.logw_ref), custom_call_target="tpu_custom_call" | custom-call | tf_op jit(solution)/shard_map/flush/pallas_call | solution.py:722
